TPU v7x, 512 devices: a whole 4x8x8 slice. The times are simulated.
512 devices in a mesh: sp: 64 (over z, y), fs: 4 (over x), tp: 2 (over core).
Axes of the slice: x: 4, y: 8, z: 8, core: 2. Of those that a mesh axis runs over, the one named last changes fastest.
Arguments:
- state_head_inputs: bfloat16 [4, 8192, 1024], P('fs', 'sp', 'tp'), may hold values from -6 to 6
- state_write_vectors: bfloat16 [4, 8192, 256], P('fs', 'sp', 'tp'), may hold values from -3 to 3
- state_read_vectors: bfloat16 [4, 8192, 256], P('fs', 'sp', 'tp'), may hold values from -3 to 3
- state_output_gate: bfloat16 [4, 8192, 1024], P('fs', 'sp', 'tp'), may hold values from -6 to 6
- presoftplus_steps: float32 [4, 16, 8192], P('fs', 'tp', 'sp'), may hold values from -6 to 6
- extra_decay_log: float32 [4, 16, 8192], P('fs', 'tp', 'sp'), may hold values from -2.1 to 0, as said below
- lane_shrinkage_powers: float32 [16], P('tp')
- bypass_coefficient_vector: float32 [16], P('tp'), may hold values from 0.5 to 4
- feeder_smoothing_stencil: bfloat16 [4, 1024], P(None, 'tp'), may hold values from -3 to 3
- stored_smoothing_stencil: bfloat16 [4, 256], P(None, 'tp'), may hold values from -3 to 3
- lookup_smoothing_stencil: bfloat16 [4, 256], P(None, 'tp'), may hold values from -3 to 3
- bundled_rescaling_vector: float32 [1024], P('tp'), may hold values from 0.1 to 1.9
- queries: bfloat16 [4, 8192, 1024], P('fs', 'sp', 'tp'), may hold values from -8 to 8
- attention_keys: bfloat16 [4, 8192, 256], P('fs', 'sp', 'tp'), may hold values from -8 to 8
- attention_values: bfloat16 [4, 8192, 256], P('fs', 'sp', 'tp'), may hold values from -6 to 6
- forget_gate_cumsum: float32 [4, 8192, 16], P('fs', 'sp', 'tp'), as said below
- state_out_weight: bfloat16 [1024, 2048], P('tp', 'fs'), may hold values from -0.1875 to 0.1875
- attention_out_weight: bfloat16 [1024, 2048], P('tp', 'fs'), may hold values from -0.75 to 0.75
Outputs:
- layer_output: bfloat16 [4, 8192, 2048], P('fs', ('sp', 'tp'))
Inputs may be any that keep to these rules, and one draw needn't show every extreme that they name: `extra_decay_log`: nonpositive. `forget_gate_cumsum`: never rises along the positions of a sequence.
All inputs are finite; a program needn't handle non-finite values.
Results may differ from a plain program's by a relative error of at most 0.019.
Values may be sent and summed in bfloat16 or wider, within the bound.
A program may use at most 64 MiB of HBM per device.

v0:
```python
import math

import jax
import jax.numpy as jnp
from jax import lax
from jax.sharding import Mesh
from jax.sharding import PartitionSpec as P

HEAD_DIM = 64
STATE = 128
SP = ("sp_0", "sp_1")
SP_TP = ("sp_0", "sp_1", "tp")


EPSILON = 1e-06
NEGATIVE = -1e30


def passed_along(shard, axis, by):
    devices = lax.axis_size(axis)
    pairs = [(i, i + by) for i in range(devices) if 0 <= i + by < devices]
    return lax.ppermute(shard, axis, pairs)


def filled_with(shard, identity):
    return jax.tree.map(
        lambda a, e: jnp.broadcast_to(jnp.asarray(e, a.dtype), a.shape), shard, identity
    )


def entering(shard, axes, combine, identity):
    before = start = filled_with(shard, identity)
    so_far = shard
    for axis in reversed(axes):
        devices, place = (lax.axis_size(axis), lax.axis_index(axis))
        pieces = jax.tree.map(
            lambda part, kind: lax.all_gather(part.astype(kind), axis),
            so_far,
            (jnp.bfloat16, jnp.bfloat16),
        )
        inside, so_far = (start, start)
        for k in range(devices):
            passed = k < place
            so_far = combine(
                so_far, jax.tree.map(lambda part, own: part[k].astype(own.dtype), pieces, shard)
            )
            inside = jax.tree.map(lambda new, old: jnp.where(passed, new, old), so_far, inside)
        before = combine(inside, before)
    return before


def in_one_piece(arrays, axis, dim, along):
    both = jnp.concatenate(arrays, axis=along)
    filled, at, outs = (lax.all_gather(both, axis, axis=dim, tiled=True), 0, [])
    for a in arrays:
        outs.append(lax.slice_in_dim(filled, at, at + a.shape[along], axis=along))
        at += a.shape[along]
    return tuple(outs)


def in_blocks(shard, dim, devices):
    before, after = (shard.shape[:dim], shard.shape[dim + 1 :])
    return jnp.moveaxis(shard.reshape(*before, devices, -1, *after), dim, 0)


def summed_on_arrival(shard, axis, dim):
    pieces = in_blocks(shard, dim, lax.axis_size(axis))
    arrived = lax.all_to_all(pieces, axis, split_axis=0, concat_axis=0, tiled=True)
    return arrived.astype(jnp.float32).sum(axis=0)


def causal_filter(feeder_quantities, before, taps):
    length = feeder_quantities.shape[0]
    padded = jnp.concatenate([before, feeder_quantities], axis=0).astype(jnp.float32)
    summed = jnp.zeros(feeder_quantities.shape, jnp.float32)
    for offset in range(taps.shape[0]):
        summed = summed + taps[offset].astype(jnp.float32) * padded[offset : offset + length]
    return jax.nn.silu(summed).astype(jnp.bfloat16)


def compose(earlier, later):
    return (earlier[0] * later[0], earlier[1] * later[0][..., None, None] + later[1])


def shards(
    state_head_inputs,
    state_write_vectors,
    state_read_vectors,
    state_output_gate,
    presoftplus_steps,
    extra_decay_log,
    lane_shrinkage_powers,
    bypass_coefficient_vector,
    feeder_smoothing_stencil,
    stored_smoothing_stencil,
    lookup_smoothing_stencil,
    bundled_rescaling_vector,
    queries,
    attention_keys,
    attention_values,
    forget_gate_cumsum,
    state_out_weight,
    attention_out_weight,
):
    shard_rows = state_head_inputs.shape[1]
    input_rows = state_head_inputs[0]
    write_rows = state_write_vectors[0]
    read_rows = state_read_vectors[0]
    tap_rows = feeder_smoothing_stencil.shape[0] - 1
    value_width = input_rows.shape[1]
    vector_width = write_rows.shape[1]
    tail_rows = jnp.concatenate(
        [input_rows[-tap_rows:], write_rows[-tap_rows:], read_rows[-tap_rows:]], axis=1
    )
    before = passed_along(tail_rows, SP, 1)
    conv_values = causal_filter(input_rows, before[:, :value_width], feeder_smoothing_stencil)
    conv_write = causal_filter(
        write_rows, before[:, value_width : value_width + vector_width], stored_smoothing_stencil
    )
    conv_read = causal_filter(
        read_rows, before[:, value_width + vector_width :], lookup_smoothing_stencil
    )
    stride_duration = jax.nn.softplus(presoftplus_steps[0])
    shrinkage_natural_power = (
        stride_duration * (-jnp.exp(lane_shrinkage_powers))[:, None] + extra_decay_log[0]
    )
    lane_tally = stride_duration.shape[0]
    groups = vector_width // STATE
    per_group = lane_tally // groups
    cumulative = jnp.cumsum(shrinkage_natural_power, axis=1)
    input_heads = conv_values.reshape(shard_rows, groups, per_group, HEAD_DIM)
    write_groups = conv_write.reshape(shard_rows, groups, STATE)
    read_groups = conv_read.reshape(shard_rows, groups, STATE)
    inner_products = jnp.einsum(
        "tgn,sgn->gts", read_groups, write_groups, preferred_element_type=jnp.float32
    )
    positions = jnp.arange(shard_rows)
    causal = positions[:, None] >= positions[None, :]
    log_gap = jnp.where(causal[None], cumulative[:, :, None] - cumulative[:, None, :], -jnp.inf)
    weights = jnp.exp(log_gap) * stride_duration[:, None, :]
    mix_weights = (
        inner_products[:, None] * weights.reshape(groups, per_group, shard_rows, shard_rows)
    ).astype(jnp.bfloat16)
    local_part = jnp.einsum(
        "ghts,sghp->tghp", mix_weights, input_heads, preferred_element_type=jnp.float32
    )
    end_scale = (jnp.exp(cumulative[:, -1:] - cumulative) * stride_duration).T.reshape(
        shard_rows, groups, per_group
    )
    weighted = (input_heads.astype(jnp.float32) * end_scale[..., None]).astype(jnp.bfloat16)
    block_state = jnp.einsum(
        "sghp,sgn->ghpn", weighted, write_groups, preferred_element_type=jnp.float32
    )
    total_decay = jnp.exp(cumulative[:, -1]).reshape(groups, per_group)
    identity = (jnp.ones_like(total_decay), jnp.zeros_like(block_state))
    carried = entering((total_decay, block_state), SP, compose, identity)[1]
    carried_part = jnp.einsum(
        "tgn,ghpn->tghp",
        read_groups,
        carried.astype(jnp.bfloat16),
        preferred_element_type=jnp.float32,
    )
    carried_part = (
        carried_part * jnp.exp(cumulative).T.reshape(shard_rows, groups, per_group)[..., None]
    )
    mixer_sum = (
        local_part
        + carried_part
        + bypass_coefficient_vector.reshape(groups, per_group)[None, :, :, None]
        * input_heads.astype(jnp.float32)
    )
    gated_rows = mixer_sum.reshape(shard_rows, groups, per_group * HEAD_DIM) * jax.nn.silu(
        state_output_gate[0].astype(jnp.float32)
    ).reshape(shard_rows, groups, -1)
    stretch_coefficient = lax.rsqrt(
        jnp.mean(gated_rows * gated_rows, axis=-1, keepdims=True) + EPSILON
    )
    state_result = (
        (gated_rows * stretch_coefficient * bundled_rescaling_vector.reshape(groups, -1))
        .reshape(shard_rows, -1)
        .astype(jnp.bfloat16)
    )
    attend_heads = forget_gate_cumsum.shape[2]
    key_group_count = attention_keys.shape[2] // HEAD_DIM
    repeat_factor = attend_heads // key_group_count
    query_head_count = queries[0].reshape(shard_rows, key_group_count, repeat_factor, HEAD_DIM)
    first_query = lax.axis_index(SP) * shard_rows
    query_index = first_query + jnp.arange(shard_rows)
    last_query = first_query + shard_rows - 1
    query_gates = forget_gate_cumsum[0].T
    all_gates = lax.all_gather(forget_gate_cumsum[0], SP, axis=0, tiled=True)
    attention_score_scale = HEAD_DIM ** (-0.5)
    starting = (
        jnp.full((attend_heads, shard_rows), NEGATIVE, jnp.float32),
        jnp.zeros((attend_heads, shard_rows), jnp.float32),
        jnp.zeros((attend_heads, shard_rows, HEAD_DIM), jnp.float32),
    )
    key_rows, value_rows = in_one_piece((attention_keys[0], attention_values[0]), SP, 0, 1)
    span = key_rows.shape[0]
    sub_block = math.gcd(span, 512)

    def advance(sub_index, running):
        first_key = sub_index * sub_block

        def attend(running):
            running_max, running_sum, weighted_sum = running
            key_tile = lax.dynamic_slice_in_dim(
                key_rows, sub_index * sub_block, sub_block, 0
            ).reshape(sub_block, key_group_count, HEAD_DIM)
            value_tile = lax.dynamic_slice_in_dim(
                value_rows, sub_index * sub_block, sub_block, 0
            ).reshape(sub_block, key_group_count, HEAD_DIM)
            key_gates = lax.dynamic_slice_in_dim(all_gates, first_key, sub_block, 0)
            attention_scores = jnp.einsum(
                "ezxp,czp->zxec", query_head_count, key_tile, preferred_element_type=jnp.float32
            )
            attention_scores = (
                attention_scores.reshape(attend_heads, shard_rows, sub_block)
                * attention_score_scale
            )
            attention_scores = attention_scores + query_gates[:, :, None] - key_gates.T[:, None, :]
            visible = (first_key + jnp.arange(sub_block))[None, :] <= query_index[:, None]
            attention_scores = jnp.where(visible[None], attention_scores, NEGATIVE)
            new_max = jnp.maximum(running_max, jnp.max(attention_scores, axis=-1))
            shrink = jnp.exp(running_max - new_max)
            attention_probs = jnp.where(
                visible[None], jnp.exp(attention_scores - new_max[..., None]), 0.0
            )
            running_sum = running_sum * shrink + jnp.sum(attention_probs, axis=-1)
            weighted_value_sum = jnp.einsum(
                "fljx,xfc->fljc",
                attention_probs.astype(jnp.bfloat16).reshape(
                    key_group_count, repeat_factor, shard_rows, sub_block
                ),
                value_tile,
                preferred_element_type=jnp.float32,
            )
            weighted_sum = weighted_sum * shrink[..., None] + weighted_value_sum.reshape(
                attend_heads, shard_rows, HEAD_DIM
            )
            return (new_max, running_sum, weighted_sum)

        return lax.cond(first_key <= last_query, attend, lambda kept: kept, running)

    _, running_sum, weighted_sum = lax.fori_loop(0, span // sub_block, advance, starting)
    attend_out = (
        (weighted_sum / running_sum[..., None])
        .transpose(1, 0, 2)
        .reshape(shard_rows, -1)
        .astype(jnp.bfloat16)
    )
    kept_rows = shard_rows // lax.axis_size("tp")
    state_all, attend_all = (
        lax.all_gather(state_result[None], "fs", axis=0, tiled=True),
        lax.all_gather(attend_out[None], "fs", axis=0, tiled=True),
    )
    sequence_count = state_all.shape[0]
    merged = jnp.einsum(
        "ftc,cd->tfd", state_all, state_out_weight, preferred_element_type=jnp.float32
    ) + jnp.einsum(
        "ftc,cd->tfd", attend_all, attention_out_weight, preferred_element_type=jnp.float32
    )
    summed = summed_on_arrival(
        merged.reshape(kept_rows * lax.axis_size("tp"), -1).astype(jnp.bfloat16), "tp", 0
    ).astype(jnp.bfloat16)
    returned = lax.all_to_all(
        summed.reshape(kept_rows, sequence_count, -1), "fs", split_axis=1, concat_axis=2, tiled=True
    )
    return returned.reshape(1, kept_rows, -1)


def solution(mesh):
    split = Mesh(
        mesh.devices.reshape(8, 8, mesh.shape["fs"], mesh.shape["tp"]), ("sp_0", "sp_1", "fs", "tp")
    )
    placed = (
        P("fs", SP, "tp"),
        P("fs", SP, "tp"),
        P("fs", SP, "tp"),
        P("fs", SP, "tp"),
        P("fs", "tp", SP),
        P("fs", "tp", SP),
        P("tp"),
        P("tp"),
        P(None, "tp"),
        P(None, "tp"),
        P(None, "tp"),
        P("tp"),
        P("fs", SP, "tp"),
        P("fs", SP, "tp"),
        P("fs", SP, "tp"),
        P("fs", SP, "tp"),
        P("tp", "fs"),
        P("tp", "fs"),
    )
    return jax.shard_map(
        shards, mesh=split, in_specs=placed, out_specs=P("fs", SP_TP, None), check_vma=False
    )
```

profile of v0, /device:TPU:504, one launch (start us, length us, event | category | flops | bytes accessed | tf_op | source)
XLA Modules:
  0.0 283.1 jit_solution(11057868072038748336)
XLA Ops:
  8.2 1.3 collective-permute-start
  13.9 1.0 copy.58
  14.9 1.9 collective-permute-done
  19.4 1.3 dynamic-slice
  21.8 16.2 %all-reduce = bf16[64]{0:T(256)(128)(2,1)S(1)} all-reduce(bf16[64]{0:T(256)(128)(2,1)S(1)} %dynamic-update-slice), channel_id=2, replica_groups=mesh['sp_0'=8,'sp_1'=8,'fs'=4,'tp'=2] {'sp_1'}, use_global_device_ids=true, to_apply=%add | all-reduce | flops 64 | bytes 256
  38.1 21.2 %all-gather.11.cloned.1.call-done = bf16[64,64,128]{2,1,0:T(8,128)(2,1)} async-done(((bf16[8,64,128]{2,1,0:T(8,128)(2,1)}), bf16[64,64,128]{2,1,0:T(8,128)(2,1)}) %all-gather.11.cloned.1.call-update) | async-done | bytes 1048592 | tf_op jit(solution)/shard_map/all_gather | solution.py:37
  59.3 2.3 fusion.35
  62.9 13.9 %all_gather.31 = bf16[8,1,8]{2,1,0:T(2,128)(2,1)S(1)} all-gather(bf16[1,1,8]{2,1,0:T(2,128)(2,1)S(1)} %fusion.66), channel_id=1, replica_groups=mesh['sp_0'=8,'sp_1'=8,'fs'=4,'tp'=2] {'sp_0'}, dimensions={0}, use_global_device_ids=true | all-gather | bytes 144 | tf_op jit(solution)/shard_map/all_gather | solution.py:37
  76.8 48.9 %all-gather.2 = f32[1,8192,8]{1,2,0:T(8,128)S(1)} all-gather(f32[1,128,8]{1,2,0:T(8,128)S(1)} %copy-done.7), channel_id=4, replica_groups=mesh['sp_0'=8,'sp_1'=8,'fs'=4,'tp'=2] {'sp_0','sp_1'}, dimensions={1}, use_global_device_ids=true | all-gather | bytes 266240 | tf_op jit(solution)/shard_map/all_gather | solution.py:191
  126.2 2.4 fusion.16
  129.4 13.1 %all_gather.35 = bf16[4,128,512]{2,1,0:T(8,128)(2,1)S(1)} all-gather(bf16[1,128,512]{2,1,0:T(8,128)(2,1)S(1)} %multiply_convert_fusion.2), channel_id=1, replica_groups=mesh['sp_0'=8,'sp_1'=8,'fs'=4,'tp'=2] {'fs'}, dimensions={0}, use_global_device_ids=true | all-gather | bytes 655360 | tf_op jit(solution)/shard_map/all_gather | solution.py:254
  142.9 50.5 %all-gather.9.cloned.1.call-done = bf16[8192,256]{0,1:T(8,128)(2,1)} async-done(((bf16[128,256]{0,1:T(8,128)(2,1)}), bf16[8192,256]{0,1:T(8,128)(2,1)}) %all-gather.9.cloned.1.call-update) | async-done | bytes 4194320 | tf_op jit(solution)/shard_map/all_gather | solution.py:54
  193.4 4.6 %fusion.71 = (bf16[8192,128]{0,1:T(8,128)(2,1)}, bf16[8192,128]{0,1:T(8,128)(2,1)}) fusion(bf16[8192,256]{0,1:T(8,128)(2,1)} %all-gather.9.cloned.1.call-done), kind=kLoop, calls=%fused_computation.181 | loop fusion | bytes 8388608 | tf_op jit(solution)/shard_map/slice | solution.py:56
  198.1 48.2 %while.18 = (s32[]{:T(128)}, f32[8,128]{1,0:T(8,128)S(1)}, f32[8,128]{1,0:T(8,128)S(1)}, f32[8,128,64]{1,2,0:T(8,128)S(1)}, s32[]{:T(128)}, /*index=5*/bf16[8192...) while((s32[]{:T(128)}, f32[8,128]{1,0:T(8,128)S(1)}, ...), condition=%wide.region_7.8_spmd.clone, body=%wide.region_2.7_spmd.clone.sunk | while | flops 140184192 | bytes 8677783 | solution.py:245
  198.1 3.0 %conditional.3 = ((f32[8,128]{1,0:T(8,128)S(1)}, f32[8,128]{1,0:T(8,128)S(1)}, f32[8,128,64]{1,2,0:T(8,128)S(1)})) conditional(s32[]{:T(128)} %convert_element_type.802, (f32[8,128]{1,0:T(8,128)S(1)}, f32[8,128]{1,0:T(8,128)S(1)}, f32[8,128,64]{1,2,0:T(8,128)S(1)}) %tuple.74, (s32[]{:T(128)}, s32[]{:T(128)}, s32[]{:T(128)}, ...), branch_computations={%region_3.3_spmd, %region_4.6_spmd} | conditional | flops 140184192 | bytes 8676992 | solution.py:243
  198.3 1.0 constant_dynamic-slice_fusion
  201.1 3.0 %conditional.3 = ((f32[8,128]{1,0:T(8,128)S(1)}, f32[8,128]{1,0:T(8,128)S(1)}, f32[8,128,64]{1,2,0:T(8,128)S(1)})) conditional(s32[]{:T(128)} %convert_element_type.802, (f32[8,128]{1,0:T(8,128)S(1)}, f32[8,128]{1,0:T(8,128)S(1)}, f32[8,128,64]{1,2,0:T(8,128)S(1)}) %tuple.74, (s32[]{:T(128)}, s32[]{:T(128)}, s32[]{:T(128)}, ...), branch_computations={%region_3.3_spmd, %region_4.6_spmd} | conditional | flops 140184192 | bytes 8676992 | solution.py:243
  201.4 1.0 constant_dynamic-slice_fusion
  204.1 3.0 %conditional.3 = ((f32[8,128]{1,0:T(8,128)S(1)}, f32[8,128]{1,0:T(8,128)S(1)}, f32[8,128,64]{1,2,0:T(8,128)S(1)})) conditional(s32[]{:T(128)} %convert_element_type.802, (f32[8,128]{1,0:T(8,128)S(1)}, f32[8,128]{1,0:T(8,128)S(1)}, f32[8,128,64]{1,2,0:T(8,128)S(1)}) %tuple.74, (s32[]{:T(128)}, s32[]{:T(128)}, s32[]{:T(128)}, ...), branch_computations={%region_3.3_spmd, %region_4.6_spmd} | conditional | flops 140184192 | bytes 8676992 | solution.py:243
  204.4 1.0 constant_dynamic-slice_fusion
  207.1 3.0 %conditional.3 = ((f32[8,128]{1,0:T(8,128)S(1)}, f32[8,128]{1,0:T(8,128)S(1)}, f32[8,128,64]{1,2,0:T(8,128)S(1)})) conditional(s32[]{:T(128)} %convert_element_type.802, (f32[8,128]{1,0:T(8,128)S(1)}, f32[8,128]{1,0:T(8,128)S(1)}, f32[8,128,64]{1,2,0:T(8,128)S(1)}) %tuple.74, (s32[]{:T(128)}, s32[]{:T(128)}, s32[]{:T(128)}, ...), branch_computations={%region_3.3_spmd, %region_4.6_spmd} | conditional | flops 140184192 | bytes 8676992 | solution.py:243
  207.4 1.0 constant_dynamic-slice_fusion
  210.1 3.0 %conditional.3 = ((f32[8,128]{1,0:T(8,128)S(1)}, f32[8,128]{1,0:T(8,128)S(1)}, f32[8,128,64]{1,2,0:T(8,128)S(1)})) conditional(s32[]{:T(128)} %convert_element_type.802, (f32[8,128]{1,0:T(8,128)S(1)}, f32[8,128]{1,0:T(8,128)S(1)}, f32[8,128,64]{1,2,0:T(8,128)S(1)}) %tuple.74, (s32[]{:T(128)}, s32[]{:T(128)}, s32[]{:T(128)}, ...), branch_computations={%region_3.3_spmd, %region_4.6_spmd} | conditional | flops 140184192 | bytes 8676992 | solution.py:243
  210.4 1.0 constant_dynamic-slice_fusion
  213.2 3.0 %conditional.3 = ((f32[8,128]{1,0:T(8,128)S(1)}, f32[8,128]{1,0:T(8,128)S(1)}, f32[8,128,64]{1,2,0:T(8,128)S(1)})) conditional(s32[]{:T(128)} %convert_element_type.802, (f32[8,128]{1,0:T(8,128)S(1)}, f32[8,128]{1,0:T(8,128)S(1)}, f32[8,128,64]{1,2,0:T(8,128)S(1)}) %tuple.74, (s32[]{:T(128)}, s32[]{:T(128)}, s32[]{:T(128)}, ...), branch_computations={%region_3.3_spmd, %region_4.6_spmd} | conditional | flops 140184192 | bytes 8676992 | solution.py:243
  213.4 1.0 constant_dynamic-slice_fusion
  216.2 3.0 %conditional.3 = ((f32[8,128]{1,0:T(8,128)S(1)}, f32[8,128]{1,0:T(8,128)S(1)}, f32[8,128,64]{1,2,0:T(8,128)S(1)})) conditional(s32[]{:T(128)} %convert_element_type.802, (f32[8,128]{1,0:T(8,128)S(1)}, f32[8,128]{1,0:T(8,128)S(1)}, f32[8,128,64]{1,2,0:T(8,128)S(1)}) %tuple.74, (s32[]{:T(128)}, s32[]{:T(128)}, s32[]{:T(128)}, ...), branch_computations={%region_3.3_spmd, %region_4.6_spmd} | conditional | flops 140184192 | bytes 8676992 | solution.py:243
  216.4 1.0 constant_dynamic-slice_fusion
  219.2 3.0 %conditional.3 = ((f32[8,128]{1,0:T(8,128)S(1)}, f32[8,128]{1,0:T(8,128)S(1)}, f32[8,128,64]{1,2,0:T(8,128)S(1)})) conditional(s32[]{:T(128)} %convert_element_type.802, (f32[8,128]{1,0:T(8,128)S(1)}, f32[8,128]{1,0:T(8,128)S(1)}, f32[8,128,64]{1,2,0:T(8,128)S(1)}) %tuple.74, (s32[]{:T(128)}, s32[]{:T(128)}, s32[]{:T(128)}, ...), branch_computations={%region_3.3_spmd, %region_4.6_spmd} | conditional | flops 140184192 | bytes 8676992 | solution.py:243
  219.4 1.0 constant_dynamic-slice_fusion
  222.2 3.0 %conditional.3 = ((f32[8,128]{1,0:T(8,128)S(1)}, f32[8,128]{1,0:T(8,128)S(1)}, f32[8,128,64]{1,2,0:T(8,128)S(1)})) conditional(s32[]{:T(128)} %convert_element_type.802, (f32[8,128]{1,0:T(8,128)S(1)}, f32[8,128]{1,0:T(8,128)S(1)}, f32[8,128,64]{1,2,0:T(8,128)S(1)}) %tuple.74, (s32[]{:T(128)}, s32[]{:T(128)}, s32[]{:T(128)}, ...), branch_computations={%region_3.3_spmd, %region_4.6_spmd} | conditional | flops 140184192 | bytes 8676992 | solution.py:243
  222.4 1.0 constant_dynamic-slice_fusion
  225.2 3.0 %conditional.3 = ((f32[8,128]{1,0:T(8,128)S(1)}, f32[8,128]{1,0:T(8,128)S(1)}, f32[8,128,64]{1,2,0:T(8,128)S(1)})) conditional(s32[]{:T(128)} %convert_element_type.802, (f32[8,128]{1,0:T(8,128)S(1)}, f32[8,128]{1,0:T(8,128)S(1)}, f32[8,128,64]{1,2,0:T(8,128)S(1)}) %tuple.74, (s32[]{:T(128)}, s32[]{:T(128)}, s32[]{:T(128)}, ...), branch_computations={%region_3.3_spmd, %region_4.6_spmd} | conditional | flops 140184192 | bytes 8676992 | solution.py:243
  225.4 1.0 constant_dynamic-slice_fusion
  228.2 3.0 %conditional.3 = ((f32[8,128]{1,0:T(8,128)S(1)}, f32[8,128]{1,0:T(8,128)S(1)}, f32[8,128,64]{1,2,0:T(8,128)S(1)})) conditional(s32[]{:T(128)} %convert_element_type.802, (f32[8,128]{1,0:T(8,128)S(1)}, f32[8,128]{1,0:T(8,128)S(1)}, f32[8,128,64]{1,2,0:T(8,128)S(1)}) %tuple.74, (s32[]{:T(128)}, s32[]{:T(128)}, s32[]{:T(128)}, ...), branch_computations={%region_3.3_spmd, %region_4.6_spmd} | conditional | flops 140184192 | bytes 8676992 | solution.py:243
  228.4 1.0 constant_dynamic-slice_fusion
  231.2 3.0 %conditional.3 = ((f32[8,128]{1,0:T(8,128)S(1)}, f32[8,128]{1,0:T(8,128)S(1)}, f32[8,128,64]{1,2,0:T(8,128)S(1)})) conditional(s32[]{:T(128)} %convert_element_type.802, (f32[8,128]{1,0:T(8,128)S(1)}, f32[8,128]{1,0:T(8,128)S(1)}, f32[8,128,64]{1,2,0:T(8,128)S(1)}) %tuple.74, (s32[]{:T(128)}, s32[]{:T(128)}, s32[]{:T(128)}, ...), branch_computations={%region_3.3_spmd, %region_4.6_spmd} | conditional | flops 140184192 | bytes 8676992 | solution.py:243
  231.5 1.0 constant_dynamic-slice_fusion
  234.2 3.0 %conditional.3 = ((f32[8,128]{1,0:T(8,128)S(1)}, f32[8,128]{1,0:T(8,128)S(1)}, f32[8,128,64]{1,2,0:T(8,128)S(1)})) conditional(s32[]{:T(128)} %convert_element_type.802, (f32[8,128]{1,0:T(8,128)S(1)}, f32[8,128]{1,0:T(8,128)S(1)}, f32[8,128,64]{1,2,0:T(8,128)S(1)}) %tuple.74, (s32[]{:T(128)}, s32[]{:T(128)}, s32[]{:T(128)}, ...), branch_computations={%region_3.3_spmd, %region_4.6_spmd} | conditional | flops 140184192 | bytes 8676992 | solution.py:243
  234.5 1.0 constant_dynamic-slice_fusion
  237.2 3.0 %conditional.3 = ((f32[8,128]{1,0:T(8,128)S(1)}, f32[8,128]{1,0:T(8,128)S(1)}, f32[8,128,64]{1,2,0:T(8,128)S(1)})) conditional(s32[]{:T(128)} %convert_element_type.802, (f32[8,128]{1,0:T(8,128)S(1)}, f32[8,128]{1,0:T(8,128)S(1)}, f32[8,128,64]{1,2,0:T(8,128)S(1)}) %tuple.74, (s32[]{:T(128)}, s32[]{:T(128)}, s32[]{:T(128)}, ...), branch_computations={%region_3.3_spmd, %region_4.6_spmd} | conditional | flops 140184192 | bytes 8676992 | solution.py:243
  237.5 1.0 constant_dynamic-slice_fusion
  240.3 3.0 %conditional.3 = ((f32[8,128]{1,0:T(8,128)S(1)}, f32[8,128]{1,0:T(8,128)S(1)}, f32[8,128,64]{1,2,0:T(8,128)S(1)})) conditional(s32[]{:T(128)} %convert_element_type.802, (f32[8,128]{1,0:T(8,128)S(1)}, f32[8,128]{1,0:T(8,128)S(1)}, f32[8,128,64]{1,2,0:T(8,128)S(1)}) %tuple.74, (s32[]{:T(128)}, s32[]{:T(128)}, s32[]{:T(128)}, ...), branch_computations={%region_3.3_spmd, %region_4.6_spmd} | conditional | flops 140184192 | bytes 8676992 | solution.py:243
  243.3 3.0 %conditional.3 = ((f32[8,128]{1,0:T(8,128)S(1)}, f32[8,128]{1,0:T(8,128)S(1)}, f32[8,128,64]{1,2,0:T(8,128)S(1)})) conditional(s32[]{:T(128)} %convert_element_type.802, (f32[8,128]{1,0:T(8,128)S(1)}, f32[8,128]{1,0:T(8,128)S(1)}, f32[8,128,64]{1,2,0:T(8,128)S(1)}) %tuple.74, (s32[]{:T(128)}, s32[]{:T(128)}, s32[]{:T(128)}, ...), branch_computations={%region_3.3_spmd, %region_4.6_spmd} | conditional | flops 140184192 | bytes 8676992 | solution.py:243
  243.5 1.0 constant_dynamic-slice_fusion
  246.4 13.1 %all_gather.38 = bf16[4,128,512]{2,1,0:T(8,128)(2,1)S(1)} all-gather(bf16[1,128,512]{2,1,0:T(8,128)(2,1)S(1)} %copy.66), channel_id=1, replica_groups=mesh['sp_0'=8,'sp_1'=8,'fs'=4,'tp'=2] {'fs'}, dimensions={0}, use_global_device_ids=true | all-gather | bytes 655360 | tf_op jit(solution)/shard_map/all_gather | solution.py:255
  260.8 4.2 %all_to_all.14 = bf16[2,64,2048]{2,1,0:T(8,128)(2,1)S(1)} all-to-all(bf16[2,64,2048]{2,1,0:T(8,128)(2,1)S(1)} %convert_element_type.644), channel_id=1, replica_groups=mesh['sp_0'=8,'sp_1'=8,'fs'=4,'tp'=2] {'tp'}, dimensions={0} | all-to-all | bytes 1048576 | tf_op jit(solution)/shard_map/all_to_all | solution.py:68
  265.1 10.4 %all_to_all.15 = bf16[64,4,512]{2,0,1:T(8,128)(2,1)S(1)} all-to-all(bf16[64,4,512]{2,0,1:T(8,128)(2,1)S(1)} %bitcast.281), channel_id=1, replica_groups=mesh['sp_0'=8,'sp_1'=8,'fs'=4,'tp'=2] {'fs'}, dimensions={1} | all-to-all | bytes 524288 | tf_op jit(solution)/shard_map/all_to_all | solution.py:266
  (293 shorter events, 45.6 us)
Async XLA Ops:
  6.5 135.9 %copy-start = (bf16[512,512]{1,0:T(8,128)(2,1)S(1)}, bf16[512,512]{1,0:T(8,128)(2,1)}, u32[]{:S(2)}) copy-start(bf16[512,512]{1,0:T(8,128)(2,1)} %param.38) | copy-start | bytes 1572868
  6.5 52.7 %all-gather.11.cloned.1.call-start = ((), (), s32[]{:S(2)}) async-start(), calls=%async_computation.4 | async-start | bytes 1179648 | tf_op jit(solution)/shard_map/all_gather | solution.py:37
  8.2 8.5 %collective-permute-start = (bf16[3,768]{0,1:T(8,128)(2,1)S(1)}, bf16[3,768]{0,1:T(8,128)(2,1)S(1)}, u32[]{:S(2)}, u32[]{:S(2)}) collective-permute-start(bf16[3,768]{0,1:T(8,128)(2,1)S(1)} %copy.57), channel_id=1, source_target_pairs={{0,8},{8,16},{16,24},{24,32},{32,40},{40,48},{48,56},{56,64},{64,7... | collective-permute-start | bytes 13832 | tf_op jit(solution)/shard_map/ppermute | solution.py:22
  17.6 44.0 %copy-start.5 = (bf16[1,128,128]{2,1,0:T(8,128)(2,1)S(1)}, bf16[1,128,128]{2,1,0:T(8,128)(2,1)}, u32[]{:S(2)}) copy-start(bf16[1,128,128]{2,1,0:T(8,128)(2,1)} %param.35) | copy-start | bytes 98308
  17.7 44.1 %copy-start.6 = (bf16[1,128,128]{2,1,0:T(8,128)(2,1)S(1)}, bf16[1,128,128]{2,1,0:T(8,128)(2,1)}, u32[]{:S(2)}) copy-start(bf16[1,128,128]{2,1,0:T(8,128)(2,1)} %param.36) | copy-start | bytes 98308
  17.8 44.7 %copy-start.3 = (bf16[1,128,512]{2,1,0:T(8,128)(2,1)S(1)}, bf16[1,128,512]{2,1,0:T(8,128)(2,1)}, u32[]{:S(2)}) copy-start(bf16[1,128,512]{2,1,0:T(8,128)(2,1)} %param.34) | copy-start | bytes 393220
  17.8 44.9 %copy-start.2 = (bf16[1,128,512]{2,1,0:T(8,128)(2,1)S(1)}, bf16[1,128,512]{2,1,0:T(8,128)(2,1)}, u32[]{:S(2)}) copy-start(bf16[1,128,512]{2,1,0:T(8,128)(2,1)} %param.25) | copy-start | bytes 393220
  17.9 58.9 %copy-start.7 = (f32[1,128,8]{1,2,0:T(8,128)S(1)}, f32[1,128,8]{1,2,0:T(8,128)}, u32[]{:S(2)}) copy-start(f32[1,128,8]{1,2,0:T(8,128)} %param.37) | copy-start | bytes 12292
  17.9 107.9 %copy-start.8 = (bf16[4,128]{1,0:T(4,128)(2,1)S(1)}, bf16[4,128]{1,0:T(4,128)(2,1)}, u32[]{:S(2)}) copy-start(bf16[4,128]{1,0:T(4,128)(2,1)} %param.32) | copy-start | bytes 3076
  17.9 108.0 %copy-start.4 = (bf16[1,128,128]{2,1,0:T(8,128)(2,1)S(1)}, bf16[1,128,128]{2,1,0:T(8,128)(2,1)}, u32[]{:S(2)}) copy-start(bf16[1,128,128]{2,1,0:T(8,128)(2,1)} %param.24) | copy-start | bytes 98308
  19.4 106.8 %all-gather.7.cloned.1.call-start = ((), (), s32[]{:S(2)}) async-start(), calls=%async_computation.2 | async-start | bytes 1179648 | tf_op jit(solution)/shard_map/all_gather | solution.py:37
  61.6 131.8 %all-gather.9.cloned.1.call-start = ((), (), s32[]{:S(2)}) async-start(), calls=%async_computation.3 | async-start | bytes 4259840 | tf_op jit(solution)/shard_map/all_gather | solution.py:54
  126.1 2.5 copy-start.10
  128.6 0.7 copy-start.9
  198.1 61.4 %copy-start.1 = (bf16[512,512]{1,0:T(8,128)(2,1)S(1)}, bf16[512,512]{1,0:T(8,128)(2,1)}, u32[]{:S(2)}) copy-start(bf16[512,512]{1,0:T(8,128)(2,1)} %param.39) | copy-start | bytes 1572868
Sparse Core Ops, SparseCore 0:
  19.5 39.7 all-gather.10
  61.7 39.5 all-gather.6
  104.3 89.0 all-gather.8
where the time goes:
time: 284 us; the launch traced here: 283 us
  blocking collectives  120 us (42%)
  waiting for transfers between devices  73.6 us (26%)
  local copies, waits for them, and re-layouts  28.3 us (10%)
  matrix products  24.3 us (9%)
  other arithmetic  19.4 us (7%)
  between operations  14.1 us (5%)
    all_gather x1, waiting for transfers between devices, in_one_piece(): filled, at, outs = (lax.all_gather(both, axis, axis=dim, tiled=True), 0, [])  50.5 us
    all_gather x1, blocking collectives, shards(): all_gates = lax.all_gather(forget_gate_cumsum[0], SP, axis=0, tiled=True)  48.9 us
    all_gather x2, waiting for transfers between devices, entering(): lax.all_gather(part.astype(kind), axis)  21.2 us
    unnamed x1, blocking collectives  16.2 us
    dynamic_slice x16, local copies, waits for them, and re-layouts, attend(): lax.dynamic_slice_in_dim(value_rows, sub_index * sub_block, sub_block, 0)  15.9 us
    all_gather x1, blocking collectives, entering(): lax.all_gather(part.astype(kind), axis)  13.9 us
    all_gather x1, blocking collectives, shards(): lax.all_gather(state_result[None], 'fs', axis=0, tiled=True)  13.1 us
    all_gather x1, blocking collectives, shards(): lax.all_gather(attend_out[None], 'fs', axis=0, tiled=True)  13.1 us
  transfers between devices with their start and end apart: 4, of which 3 were waited for; matrix products, arithmetic and copies ran while one was open for 4% of the time, Pallas kernels for 0%

commit v1 on v0

v1 whole, which is shorter than its diff:
```python
import jax
import jax.numpy as jnp
from jax import lax
from jax.experimental import pallas as pl
from jax.experimental.pallas import tpu as pltpu
from jax.sharding import Mesh
from jax.sharding import PartitionSpec as P

SP = ("sp_0", "sp_1")
SP_TP = ("sp_0", "sp_1", "tp")
MESH = pl.DeviceIdType.MESH
BF16 = jnp.bfloat16
F32 = jnp.float32

RING = 8
FS = 4
ROWS = 128
HD = 64
BLOCK = ROWS + 16
MSG = HD + 16
EPSILON = 1e-06
NEG = -1e30

NT = (((1,), (1,)), ((), ()))
TN = (((0,), (0,)), ((), ()))


def mod8(i):
    return lax.rem(i + 2 * RING, RING)


def mod4(i):
    return lax.rem(i + 2 * FS, FS)


def dot(a, b, dims=None):
    if dims is None:
        return jnp.dot(a, b, preferred_element_type=F32)
    return lax.dot_general(a, b, dims, preferred_element_type=F32)


def silu(f):
    return f / (1.0 + jnp.exp(-f))


def split3(g):
    hi = g.astype(BF16).astype(F32)
    rest = g - hi
    mid = rest.astype(BF16).astype(F32)
    return hi, mid, rest - mid


def kernel(
    x_ref, w_ref, r_ref, gate_ref, step_ref, extra_ref, lane_ref, bypass_ref,
    xtap_ref, wtap_ref, rtap_ref, gain_ref, q_ref, k_ref, v_ref, g_ref, w1_ref, w2_ref,
    out_ref,
    kv, qs, wide, hx, hw, hr, m_sc, acc_sc, msg, s1, tot, s2, pre, cumpre, back, carried,
    xs_sc, ms_sc, rd_sc, ecum_sc, wbuf, give, take,
    kv1_send, kv1_recv, kv_send, kv_recv, s1_send, s1_recv, s2_send, s2_recv, s3_send, s3_recv,
    w_send, w_recv, own_sem, halo_send, halo_recv, tp_send, tp_recv,
):
    z, y = lax.axis_index("sp_0"), lax.axis_index("sp_1")
    fx, tp = lax.axis_index("fs"), lax.axis_index("tp")
    me = z * RING + y
    maj = (z, y)
    axis_of = ("sp_0", "sp_1")
    after, before = lax.rem(me + 1, RING * RING), lax.rem(me + RING * RING - 1, RING * RING)

    def at_sp(i):
        return {"sp_0": i // RING, "sp_1": lax.rem(i, RING)}

    def remote(src, dst, send, recv, where):
        return pltpu.make_async_remote_copy(
            src_ref=src, dst_ref=dst, send_sem=send, recv_sem=recv,
            device_id=where, device_id_type=MESH,
        )

    lane = lax.broadcasted_iota(jnp.int32, (ROWS, ROWS), 1)
    sub = lax.broadcasted_iota(jnp.int32, (ROWS, ROWS), 0)
    low = lane < HD
    sub8 = lax.broadcasted_iota(jnp.int32, (8, ROWS), 0)

    kf, vf = k_ref[...].astype(F32), v_ref[...].astype(F32)
    both = (
        jnp.where(low, kf, pltpu.roll(vf, HD, 1)).astype(BF16),
        jnp.where(low, pltpu.roll(kf, HD, 1), vf).astype(BF16),
    )
    wide[...] = jnp.zeros_like(wide)
    wide[:, 0:8] = g_ref[...]
    gt = wide[...].T[0:8]
    hi, mid, lo = split3(gt)
    four = sub8 < 4
    rows0 = jnp.concatenate(
        [jnp.where(four, hi, pltpu.roll(lo, 4, 0)), jnp.where(four, mid, 0.0)], axis=0
    )
    rows1 = jnp.concatenate(
        [jnp.where(four, pltpu.roll(hi, 4, 0), lo), jnp.where(four, pltpu.roll(mid, 4, 0), 0.0)], axis=0
    )
    kv[0, z, y, 0:ROWS] = both[0]
    kv[1, y, z, 0:ROWS] = both[1]
    kv[0, z, y, ROWS:BLOCK] = rows0.astype(BF16)
    kv[1, y, z, ROWS:BLOCK] = rows1.astype(BF16)
    for p in range(4):
        qf = q_ref[:, 128 * p : 128 * p + 128].astype(F32) * 0.125
        qs[2 * p] = jnp.where(low, qf, 0.0).astype(BF16)
        qs[2 * p + 1] = jnp.where(low, pltpu.roll(qf, HD, 1), 0.0).astype(BF16)

    barrier = pltpu.get_barrier_semaphore()
    peers = [{"sp_1": mod8(y + d)} for d in range(1, RING)]
    peers += [{"sp_0": mod8(z + d)} for d in range(1, RING)]
    peers += [{"fs": mod4(fx + 1)}, {"fs": mod4(fx - 1)}, {"tp": 1 - tp}]
    peers += [at_sp(after), at_sp(before)]
    for peer in peers:
        pl.semaphore_signal(barrier, inc=1, device_id=peer, device_id_type=MESH)
    pl.semaphore_wait(barrier, len(peers))

    halos = []
    for i, (src, dst) in enumerate(((x_ref, hx), (w_ref, hw), (r_ref, hr))):
        halos.append(
            remote(src.at[pl.ds(ROWS - 16, 16)], dst, halo_send.at[i], halo_recv.at[i], at_sp(after))
        )
        halos[-1].start()

    def first(c, d):
        peer = mod8(maj[1 - c] + d)
        own = kv.at[c, maj[c], maj[1 - c]]
        return remote(own, own, kv1_send.at[c, d], kv1_recv.at[c, RING - d],
                      {axis_of[1 - c]: peer})

    def first_arrival(c, d):
        peer = mod8(maj[1 - c] + d)
        slot = kv.at[c, maj[c], peer]
        return remote(slot, slot, kv1_send.at[c, d], kv1_recv.at[c, d], {axis_of[1 - c]: peer})

    for d in range(1, RING):
        for c in range(2):
            first(c, d).start()

    right, left = {"fs": mod4(fx + 1)}, {"fs": mod4(fx - 1)}
    owns = [
        pltpu.make_async_copy(w1_ref, wbuf.at[0, fx], own_sem.at[0]),
        pltpu.make_async_copy(w2_ref, wbuf.at[1, fx], own_sem.at[1]),
    ]

    def weights(j, d):
        src = (w1_ref, w2_ref)[j]
        return remote(src, wbuf.at[j, fx], w_send.at[j, d], w_recv.at[j, d], (right, left)[d])

    def weights_arrival(j, d):
        slot = wbuf.at[j, mod4(fx - 1) if d == 0 else mod4(fx + 1)]
        return remote(slot, slot, w_send.at[j, d], w_recv.at[j, d], (right, left)[d])

    def passed_on(j):
        slot = wbuf.at[j, mod4(fx - 1) if j == 0 else mod4(fx + 1)]
        return remote(slot, slot, w_send.at[j, 2], w_recv.at[j, 2], (right, left)[j])

    def passed_arrival(j):
        slot = wbuf.at[j, mod4(fx + 2)]
        return remote(slot, slot, w_send.at[j, 2], w_recv.at[j, 2], (right, left)[j])

    for o in owns:
        o.start()
    for j in range(2):
        for d in range(2):
            weights(j, d).start()

    for h in range(8):
        c = h // 4
        own = both[c]
        s = dot(qs[h], own, NT) - gt[h : h + 1, :]
        s = jnp.where(lane <= sub, s, NEG)
        m = jnp.max(s, axis=1, keepdims=True)
        p = jnp.exp(s - m)
        m_sc[h] = jnp.broadcast_to(m, (ROWS, ROWS))
        acc_sc[h] = dot(p.astype(BF16), jnp.where(low, 1.0, own.astype(F32)).astype(BF16))

    for h in halos:
        h.wait_recv()
    opening = me > 0

    def filtered(rows, halo, taps):
        old = jnp.where(opening, halo[...].astype(F32), 0.0)
        padded = jnp.concatenate([old, rows[...].astype(F32)], axis=0)
        t = taps[...].astype(F32)
        total = t[0:1] * padded[13 : 13 + ROWS]
        for o in range(1, 4):
            total = total + t[o : o + 1] * padded[13 + o : 13 + o + ROWS]
        return silu(total).astype(BF16)

    xs_sc[...] = filtered(x_ref, hx, xtap_ref)
    wr = filtered(w_ref, hw, wtap_ref)
    rd = filtered(r_ref, hr, rtap_ref)
    rd_sc[...] = rd
    raw = step_ref[...]
    step = jnp.maximum(raw, 0.0) + jnp.log1p(jnp.exp(-jnp.abs(raw)))
    rate = jnp.zeros((8, ROWS), F32)
    for h in range(8):
        rate = jnp.where(sub8 == h, lane_ref[h], rate)
    cum = step * (-jnp.exp(rate)) + extra_ref[...]
    lane8 = lax.broadcasted_iota(jnp.int32, (8, ROWS), 1)
    for shift in (1, 2, 4, 8, 16, 32, 64):
        cum = cum + jnp.where(lane8 >= shift, pltpu.roll(cum, shift, 1), 0.0)
    end = cum[:, ROWS - 1 : ROWS]
    scale = jnp.exp(end - cum) * step
    wide[0:8] = cum
    wide[8:16] = scale
    wide[16:24] = jnp.broadcast_to(end, (8, ROWS))
    turned = wide[...].T
    inner = dot(rd, wr, NT)
    causal = lane <= sub
    for p in range(4):
        xp = xs_sc[:, 128 * p : 128 * p + 128]
        parts = []
        for e in range(2):
            h = 2 * p + e
            gap = jnp.where(causal, turned[:, h : h + 1] - cum[h : h + 1, :], NEG)
            mix = inner * (jnp.exp(gap) * step[h : h + 1, :])
            parts.append(dot(mix.astype(BF16), xp))
        xf = xp.astype(F32)
        skip = jnp.where(low, bypass_ref[2 * p], bypass_ref[2 * p + 1])
        ms_sc[:, 128 * p : 128 * p + 128] = jnp.where(low, parts[0], parts[1]) + skip * xf
        ends = jnp.where(low, turned[:, 8 + 2 * p : 9 + 2 * p], turned[:, 9 + 2 * p : 10 + 2 * p])
        ecum_sc[:, 128 * p : 128 * p + 128] = jnp.exp(
            jnp.where(low, turned[:, 2 * p : 2 * p + 1], turned[:, 2 * p + 1 : 2 * p + 2])
        )
        state = dot((xf * ends).astype(BF16), wr, TN)
        for e in range(2):
            h = 2 * p + e
            msg[h, 0:HD] = state[HD * e : HD * e + HD].astype(BF16)

    def decay_rows(total):
        a, b, c3 = split3(total)
        return jnp.concatenate([jnp.where(four, a, c3), b], axis=0).astype(BF16)

    def decay_of(rows):
        f = rows.astype(F32)
        return (f[0:1] + f[8:9]) + f[4:5]

    for h in range(8):
        msg[h, HD:MSG] = decay_rows(jnp.broadcast_to(end[h : h + 1], (8, ROWS)))

    def around(src, dst, send, recv, axis, d):
        me_on = y if axis == "sp_1" else z
        peer = mod8(me_on + d)
        return remote(src(peer), dst.at[me_on], send.at[d], recv.at[RING - d], {axis: peer})

    def around_arrival(dst, send, recv, axis, d):
        me_on = y if axis == "sp_1" else z
        peer = mod8(me_on + d)
        slot = dst.at[peer]
        return remote(slot, slot, send.at[d], recv.at[d], {axis: peer})

    s1_out = [around(lambda p: msg.at[p], s1, s1_send, s1_recv, "sp_1", d) for d in range(1, RING)]
    for o in s1_out:
        o.start()
    s1[y] = msg[y]

    def bundle(c, row, half):
        return kv.at[c, row, pl.ds(4 * half, 4)]

    def hop(c, d, k):
        away = -(k // 2) if d == 0 else k // 2
        half = (0 if d == 0 else 1) if k == 6 else k % 2
        slot = bundle(c, mod8(maj[c] + away), half)
        to = mod8(maj[c] + (1 if d == 0 else -1))
        return remote(slot, slot, kv_send.at[c, d, k], kv_recv.at[c, d, k], {axis_of[c]: to})

    def hop_arrival(c, d, k):
        away = -(k // 2) - 1 if d == 0 else k // 2 + 1
        half = (0 if d == 0 else 1) if k == 6 else k % 2
        slot = bundle(c, mod8(maj[c] + away), half)
        to = mod8(maj[c] + (1 if d == 0 else -1))
        return remote(slot, slot, kv_send.at[c, d, k], kv_recv.at[c, d, k], {axis_of[c]: to})

    def attend(up, down, half_up, half_down):
        def one(c, carry):
            mine = jnp.where(c == 0, z, y)
            row_u, row_d = mod8(mine + up), mod8(mine + down)
            stride = jnp.where(c == 0, RING, 1)
            inner_stride = jnp.where(c == 0, 1, RING)
            lead_u = row_u * stride + 4 * half_up * inner_stride
            lead_d = row_d * stride + 4 * half_down * inner_stride

            @pl.when(jnp.minimum(lead_u, lead_d) < me)
            def _():
                keys, bias, vals = [], [], []
                for row, half, lead in ((row_u, half_up, lead_u), (row_d, half_down, lead_d)):
                    for b in range(4):
                        rows = kv[c, row, 4 * half + b, 0:ROWS]
                        g = kv[c, row, 4 * half + b, ROWS:BLOCK].astype(F32)
                        g = g[0:8] + g[8:16]
                        g = g + pltpu.roll(g, 4, 0)
                        seen = lead + b * inner_stride < me
                        bias.append(jnp.where(seen, -g, NEG))
                        keys.append(rows)
                        vals.append(jnp.where(low, jnp.ones_like(rows), rows))
                keys = jnp.concatenate(keys, axis=0)
                vals = jnp.concatenate(vals, axis=0)
                bias = jnp.concatenate(bias, axis=1)
                for i in range(4):
                    h = 4 * c + i
                    s = dot(qs[h], keys, NT) + bias[i : i + 1, :]
                    m_old = m_sc[h]
                    m_new = jnp.maximum(m_old, jnp.max(s, axis=1, keepdims=True))
                    m_sc[h] = m_new
                    p = jnp.exp(s - m_new[:, 0:1])
                    acc_sc[h] = acc_sc[h] * jnp.exp(m_old - m_new) + dot(p.astype(BF16), vals)

            return carry

        lax.fori_loop(0, 2, one, 0)

    for d in range(1, RING):
        for c in range(2):
            first_arrival(c, d).wait_recv()
    for k in range(2):
        for c in range(2):
            for d in range(2):
                hop(c, d, k).start()
    attend(0, 0, 0, 1)

    def stage(k):
        if k == 0:
            weights_arrival(0, 0).wait_recv()
            passed_on(0).start()
        if k == 1:
            for d in range(1, RING):
                around_arrival(s1, s1_send, s1_recv, "sp_1", d).wait_recv()
            run = jnp.zeros((HD, ROWS), F32)
            total = jnp.zeros((1, ROWS), F32)
            for j in range(RING):
                pre[j] = run
                cumpre[j] = jnp.broadcast_to(total, (8, ROWS))
                ld = decay_of(s1[j, HD:MSG])
                run = jnp.exp(ld) * run + s1[j, 0:HD].astype(F32)
                total = total + ld
            tot[0:HD] = run.astype(BF16)
            tot[HD:MSG] = decay_rows(jnp.broadcast_to(total, (8, ROWS)))
            for d in range(1, RING):
                around(lambda p: tot, s2, s2_send, s2_recv, "sp_0", d).start()
        if k == 3:
            for d in range(1, RING):
                around_arrival(s2, s2_send, s2_recv, "sp_0", d).wait_recv()
            s2[z] = tot[...]
            entering = jnp.zeros((HD, ROWS), F32)
            for j in range(RING - 1):
                later = jnp.exp(decay_of(s2[j, HD:MSG])) * entering + s2[j, 0:HD].astype(F32)
                entering = jnp.where(j < z, later, entering)
            for j in range(RING):
                back[j] = (pre[j] + jnp.exp(cumpre[j, 0:1]) * entering).astype(BF16)
            for d in range(1, RING):
                around(lambda p: back.at[p], carried, s3_send, s3_recv, "sp_1", d).start()
            carried[y] = back[y]
        if k == 4:
            weights_arrival(1, 1).wait_recv()
            passed_on(1).start()
        if k == 5:
            for d in range(1, RING):
                around_arrival(carried, s3_send, s3_recv, "sp_1", d).wait_recv()
            states = jnp.concatenate([carried[h] for h in range(8)], axis=0)
            u = dot(rd_sc[...], states, NT) * ecum_sc[...] + ms_sc[...]
            u = u * silu(gate_ref[...].astype(F32))
            stretch = lax.rsqrt(jnp.mean(u * u, axis=1, keepdims=True) + EPSILON)
            xs_sc[...] = (u * stretch * gain_ref[...]).astype(BF16)

    for k in range(7):
        for c in range(2):
            for d in range(2):
                hop_arrival(c, d, k).wait_recv()
        for c in range(2):
            if k < 5:
                hop(c, 0, k + 2).start()
            if k < 4:
                hop(c, 1, k + 2).start()
            if k == 5:
                hop(c, 1, 6).start()
        half_up = 0 if k == 6 else k % 2
        half_down = 1 if k == 6 else k % 2
        attend(-(k // 2) - 1, k // 2 + 1, half_up, half_down)
        stage(k)

    attended = []
    for p in range(4):
        a, b = acc_sc[2 * p], acc_sc[2 * p + 1]
        first_half = pltpu.roll(a, HD, 1) / a
        second_half = b / pltpu.roll(b, HD, 1)
        attended.append(jnp.where(low, first_half, second_half).astype(BF16))
    attended = jnp.concatenate(attended, axis=1)
    state_out = xs_sc[...]
    for o in owns:
        o.wait()
    weights_arrival(0, 1).wait_recv()
    weights_arrival(1, 0).wait_recv()
    for j in range(2):
        passed_arrival(j).wait_recv()
    whole = []
    half_rows = ROWS // 2
    for f in range(FS):
        merged = dot(state_out, wbuf[0, f]) + dot(attended, wbuf[1, f])
        top, bottom = merged[0:half_rows], merged[half_rows:ROWS]
        give[f] = jnp.where(tp == 0, bottom, top).astype(BF16)
        copy = remote(give.at[f], take.at[f], tp_send.at[f], tp_recv.at[f], {"tp": 1 - tp})
        copy.start()
        whole.append(jnp.where(tp == 0, top, bottom))
    for f in range(FS):
        copy = remote(give.at[f], take.at[f], tp_send.at[f], tp_recv.at[f], {"tp": 1 - tp})
        copy.wait_recv()
        out_ref[:, 512 * f : 512 * f + 512] = (whole[f] + take[f].astype(F32)).astype(BF16)

    for f in range(FS):
        remote(give.at[f], take.at[f], tp_send.at[f], tp_recv.at[f], {"tp": 1 - tp}).wait_send()
    for h in halos:
        h.wait_send()
    for d in range(1, RING):
        for c in range(2):
            first(c, d).wait_send()
        around(lambda p: msg.at[p], s1, s1_send, s1_recv, "sp_1", d).wait_send()
        around(lambda p: tot, s2, s2_send, s2_recv, "sp_0", d).wait_send()
        around(lambda p: back.at[p], carried, s3_send, s3_recv, "sp_1", d).wait_send()
    for k in range(7):
        for c in range(2):
            for d in range(2):
                hop(c, d, k).wait_send()
    for j in range(2):
        for d in range(2):
            weights(j, d).wait_send()
        passed_on(j).wait_send()


def shards(
    state_head_inputs, state_write_vectors, state_read_vectors, state_output_gate,
    presoftplus_steps, extra_decay_log, lane_shrinkage_powers, bypass_coefficient_vector,
    feeder_smoothing_stencil, stored_smoothing_stencil, lookup_smoothing_stencil,
    bundled_rescaling_vector, queries, attention_keys, attention_values, forget_gate_cumsum,
    state_out_weight, attention_out_weight,
):
    vmem = pl.BlockSpec(memory_space=pltpu.VMEM)
    smem = pl.BlockSpec(memory_space=pltpu.SMEM)
    anyw = pl.BlockSpec(memory_space=pl.ANY)
    dma = pltpu.SemaphoreType.DMA
    out = pl.pallas_call(
        kernel,
        out_shape=jax.ShapeDtypeStruct((ROWS // 2, 512 * FS), BF16),
        in_specs=[vmem] * 6 + [smem] * 2 + [vmem] * 8 + [anyw] * 2,
        out_specs=vmem,
        scratch_shapes=[
            pltpu.VMEM((2, RING, RING, BLOCK, ROWS), BF16),
            pltpu.VMEM((8, ROWS, ROWS), BF16),
            pltpu.VMEM((ROWS, ROWS), F32),
            pltpu.VMEM((16, 512), BF16),
            pltpu.VMEM((16, ROWS), BF16),
            pltpu.VMEM((16, ROWS), BF16),
            pltpu.VMEM((8, ROWS, ROWS), F32),
            pltpu.VMEM((8, ROWS, ROWS), F32),
            pltpu.VMEM((RING, MSG, ROWS), BF16),
            pltpu.VMEM((RING, MSG, ROWS), BF16),
            pltpu.VMEM((MSG, ROWS), BF16),
            pltpu.VMEM((RING, MSG, ROWS), BF16),
            pltpu.VMEM((RING, HD, ROWS), F32),
            pltpu.VMEM((RING, 8, ROWS), F32),
            pltpu.VMEM((RING, HD, ROWS), BF16),
            pltpu.VMEM((RING, HD, ROWS), BF16),
            pltpu.VMEM((ROWS, 512), BF16),
            pltpu.VMEM((ROWS, 512), F32),
            pltpu.VMEM((ROWS, ROWS), BF16),
            pltpu.VMEM((ROWS, 512), F32),
            pltpu.VMEM((2, FS, 512, 512), BF16),
            pltpu.VMEM((FS, ROWS // 2, 512), BF16),
            pltpu.VMEM((FS, ROWS // 2, 512), BF16),
            dma((2, RING)), dma((2, RING)),
            dma((2, 2, 7)), dma((2, 2, 7)),
            dma((RING,)), dma((RING,)), dma((RING,)), dma((RING,)), dma((RING,)), dma((RING,)),
            dma((2, 3)), dma((2, 3)), dma((2,)),
            dma((3,)), dma((3,)), dma((FS,)), dma((FS,)),
        ],
        compiler_params=pltpu.CompilerParams(
            collective_id=0, has_side_effects=True, vmem_limit_bytes=48 * 1024 * 1024
        ),
        name="mixer",
    )(
        state_head_inputs[0], state_write_vectors[0], state_read_vectors[0], state_output_gate[0],
        presoftplus_steps[0], extra_decay_log[0], lane_shrinkage_powers, bypass_coefficient_vector,
        feeder_smoothing_stencil, stored_smoothing_stencil, lookup_smoothing_stencil,
        bundled_rescaling_vector.reshape(1, -1), queries[0], attention_keys[0], attention_values[0],
        forget_gate_cumsum[0], state_out_weight, attention_out_weight,
    )
    return out[None]


def solution(mesh):
    split = Mesh(
        mesh.devices.reshape(8, 8, mesh.shape["fs"], mesh.shape["tp"]), ("sp_0", "sp_1", "fs", "tp")
    )
    placed = (
        P("fs", SP, "tp"),
        P("fs", SP, "tp"),
        P("fs", SP, "tp"),
        P("fs", SP, "tp"),
        P("fs", "tp", SP),
        P("fs", "tp", SP),
        P("tp"),
        P("tp"),
        P(None, "tp"),
        P(None, "tp"),
        P(None, "tp"),
        P("tp"),
        P("fs", SP, "tp"),
        P("fs", SP, "tp"),
        P("fs", SP, "tp"),
        P("fs", SP, "tp"),
        P("tp", "fs"),
        P("tp", "fs"),
    )
    return jax.shard_map(
        shards, mesh=split, in_specs=placed, out_specs=P("fs", SP_TP, None), check_vma=False
    )
```

time: 284 us -> 72.6 us (0.26)
  the two profiles are of different devices: /device:TPU:504 before, /device:TPU:59 now
where the time goes in v1:
time: 72.6 us; the launch traced here: 72.1 us
  Pallas kernels  63.6 us (88%)
  local copies, waits for them, and re-layouts  8.4 us (12%)
    pallas_call x1, Pallas kernels, shards(): pl.pallas_call(kernel, out_shape=jax.ShapeDtypeStruct((ROWS // 2, 512 * F...  63.6 us
    unnamed x38, local copies, waits for them, and re-layouts  8.4 us

profile of v1, /device:TPU:59, one launch (start us, length us, event | category | flops | bytes accessed | tf_op | source)
XLA Modules:
  0.0 72.1 jit_solution(6970791263485292757)
XLA Ops:
  0.0 0.0 copy-start.17
  0.0 0.0 copy-start.14
  0.0 0.0 copy-start.15
  0.0 0.0 copy-start.16
  0.0 0.0 copy-start.12
  0.0 0.0 copy-start.11
  0.0 0.0 copy-start.10
  0.0 0.6 copy-done.17
  0.7 0.0 copy-start.5
  0.7 0.0 copy-start.6
  0.7 0.0 copy-start.9
  0.7 0.1 copy.19
  0.8 0.0 copy-start.13
  0.8 0.0 copy-done.14
  0.8 0.0 copy-done.15
  0.8 0.0 copy-done.16
  0.8 0.0 copy-done.12
  0.8 0.0 copy-done.11
  0.9 0.0 copy-done.10
  0.9 0.6 copy-done.5
  1.4 0.0 copy-done.6
  1.5 0.0 copy-done.9
  1.5 0.0 copy-done.13
  1.5 0.0 copy-start
  1.5 1.0 %copy-done = bf16[512,512]{1,0:T(8,128)(2,1)S(1)} copy-done((bf16[512,512]{1,0:T(8,128)(2,1)S(1)}, bf16[512,512]{1,0:T(8,128)(2,1)}, u32[]{:S(2)}) %copy-start) | copy-done | bytes 524312
  2.5 0.0 copy-start.1
  2.5 1.0 %copy-done.1 = bf16[512,512]{1,0:T(8,128)(2,1)S(1)} copy-done((bf16[512,512]{1,0:T(8,128)(2,1)S(1)}, bf16[512,512]{1,0:T(8,128)(2,1)}, u32[]{:S(2)}) %copy-start.1) | copy-done | bytes 524312
  3.6 0.0 copy-start.2
  3.6 0.9 %copy-done.2 = bf16[1,128,512]{2,1,0:T(8,128)(2,1)S(1)} copy-done((bf16[1,128,512]{2,1,0:T(8,128)(2,1)S(1)}, bf16[1,128,512]{2,1,0:T(8,128)(2,1)}, u32[]{:S(2)}) %copy-start.2) | copy-done | bytes 131096
  4.5 0.0 copy-start.3
  4.5 0.9 %copy-done.3 = bf16[1,128,512]{2,1,0:T(8,128)(2,1)S(1)} copy-done((bf16[1,128,512]{2,1,0:T(8,128)(2,1)S(1)}, bf16[1,128,512]{2,1,0:T(8,128)(2,1)}, u32[]{:S(2)}) %copy-start.3) | copy-done | bytes 131096
  5.4 0.0 copy-start.4
  5.4 0.9 %copy-done.4 = bf16[1,128,512]{2,1,0:T(8,128)(2,1)S(1)} copy-done((bf16[1,128,512]{2,1,0:T(8,128)(2,1)S(1)}, bf16[1,128,512]{2,1,0:T(8,128)(2,1)}, u32[]{:S(2)}) %copy-start.4) | copy-done | bytes 131096
  6.3 0.0 copy-start.7
  6.3 0.8 %copy-done.7 = bf16[1,128,128]{2,1,0:T(8,128)(2,1)S(1)} copy-done((bf16[1,128,128]{2,1,0:T(8,128)(2,1)S(1)}, bf16[1,128,128]{2,1,0:T(8,128)(2,1)}, u32[]{:S(2)}) %copy-start.7) | copy-done | bytes 32792
  7.0 0.0 copy-start.8
  7.0 0.8 %copy-done.8 = bf16[1,128,128]{2,1,0:T(8,128)(2,1)S(1)} copy-done((bf16[1,128,128]{2,1,0:T(8,128)(2,1)S(1)}, bf16[1,128,128]{2,1,0:T(8,128)(2,1)}, u32[]{:S(2)}) %copy-start.8) | copy-done | bytes 32792
  7.8 63.6 %mixer.1 = bf16[64,2048]{1,0:T(8,128)(2,1)S(1)} custom-call(bf16[128,512]{1,0:T(8,128)(2,1)S(1)} %bitcast.14, bf16[128,128]{1,0:T(8,128)(2,1)S(1)} %bitcast.17, bf16[128,128]{1,0:T(8,128)(2,1)S(1)} %bitcast.18, bf16[128,512]{1,0:T(8,128)(2,1)S(1)} %bitcast.15, f32[8,128]{1,0:T(8,128)S(1)} %bitcast.21, f32[8,128]{1,0:T(8,128)S(1)} %bitcast.22, ...), custom_call_target="tpu_custom_call" | custom-call | tf_op jit(solution)/shard_map/mixer/pallas_call | solution.py:441
  71.4 0.7 copy.21
Async XLA Ops:
  0.0 0.7 copy-start.17
  0.0 0.8 %copy-start.14 = (bf16[4,128]{1,0:T(4,128)(2,1)S(1)}, bf16[4,128]{1,0:T(4,128)(2,1)}, u32[]{:S(2)}) copy-start(bf16[4,128]{1,0:T(4,128)(2,1)} %rtap_ref.1) | copy-start | bytes 3076
  0.0 0.8 %copy-start.15 = (f32[8]{0:T(128)S(1)}, f32[8]{0:T(128)}, u32[]{:S(2)}) copy-start(f32[8]{0:T(128)} %lane_ref.1) | copy-start | bytes 100
  0.0 0.8 %copy-start.16 = (f32[8]{0:T(128)S(1)}, f32[8]{0:T(128)}, u32[]{:S(2)}) copy-start(f32[8]{0:T(128)} %bypass_ref.1) | copy-start | bytes 100
  0.0 0.8 %copy-start.12 = (f32[512]{0:T(512)S(1)}, f32[512]{0:T(512)}, u32[]{:S(2)}) copy-start(f32[512]{0:T(512)} %param.29) | copy-start | bytes 6148
  0.0 0.8 %copy-start.11 = (bf16[4,512]{1,0:T(4,128)(2,1)S(1)}, bf16[4,512]{1,0:T(4,128)(2,1)}, u32[]{:S(2)}) copy-start(bf16[4,512]{1,0:T(4,128)(2,1)} %xtap_ref.1) | copy-start | bytes 12292
  0.0 0.8 %copy-start.10 = (f32[1,8,128]{2,1,0:T(8,128)S(1)}, f32[1,8,128]{2,1,0:T(8,128)}, u32[]{:S(2)}) copy-start(f32[1,8,128]{2,1,0:T(8,128)} %param.23) | copy-start | bytes 12292
  0.7 0.8 %copy-start.5 = (bf16[1,128,128]{2,1,0:T(8,128)(2,1)S(1)}, bf16[1,128,128]{2,1,0:T(8,128)(2,1)}, u32[]{:S(2)}) copy-start(bf16[1,128,128]{2,1,0:T(8,128)(2,1)} %param.19) | copy-start | bytes 98308
  0.7 0.8 %copy-start.6 = (bf16[1,128,128]{2,1,0:T(8,128)(2,1)S(1)}, bf16[1,128,128]{2,1,0:T(8,128)(2,1)}, u32[]{:S(2)}) copy-start(bf16[1,128,128]{2,1,0:T(8,128)(2,1)} %param.20) | copy-start | bytes 98308
  0.7 0.8 %copy-start.9 = (f32[1,8,128]{2,1,0:T(8,128)S(1)}, f32[1,8,128]{2,1,0:T(8,128)}, u32[]{:S(2)}) copy-start(f32[1,8,128]{2,1,0:T(8,128)} %param.22) | copy-start | bytes 12292
  0.8 0.7 copy-start.13
  1.5 1.0 %copy-start = (bf16[512,512]{1,0:T(8,128)(2,1)S(1)}, bf16[512,512]{1,0:T(8,128)(2,1)}, u32[]{:S(2)}) copy-start(bf16[512,512]{1,0:T(8,128)(2,1)} %w1_ref.1) | copy-start | bytes 1572868
  2.5 1.0 %copy-start.1 = (bf16[512,512]{1,0:T(8,128)(2,1)S(1)}, bf16[512,512]{1,0:T(8,128)(2,1)}, u32[]{:S(2)}) copy-start(bf16[512,512]{1,0:T(8,128)(2,1)} %w2_ref.1) | copy-start | bytes 1572868
  3.6 0.9 %copy-start.2 = (bf16[1,128,512]{2,1,0:T(8,128)(2,1)S(1)}, bf16[1,128,512]{2,1,0:T(8,128)(2,1)}, u32[]{:S(2)}) copy-start(bf16[1,128,512]{2,1,0:T(8,128)(2,1)} %param.18) | copy-start | bytes 393220
  4.5 0.9 %copy-start.3 = (bf16[1,128,512]{2,1,0:T(8,128)(2,1)S(1)}, bf16[1,128,512]{2,1,0:T(8,128)(2,1)}, u32[]{:S(2)}) copy-start(bf16[1,128,512]{2,1,0:T(8,128)(2,1)} %param.21) | copy-start | bytes 393220
  5.4 0.9 %copy-start.4 = (bf16[1,128,512]{2,1,0:T(8,128)(2,1)S(1)}, bf16[1,128,512]{2,1,0:T(8,128)(2,1)}, u32[]{:S(2)}) copy-start(bf16[1,128,512]{2,1,0:T(8,128)(2,1)} %param.30) | copy-start | bytes 393220
  6.3 0.8 %copy-start.7 = (bf16[1,128,128]{2,1,0:T(8,128)(2,1)S(1)}, bf16[1,128,128]{2,1,0:T(8,128)(2,1)}, u32[]{:S(2)}) copy-start(bf16[1,128,128]{2,1,0:T(8,128)(2,1)} %param.31) | copy-start | bytes 98308
  7.0 0.8 %copy-start.8 = (bf16[1,128,128]{2,1,0:T(8,128)(2,1)S(1)}, bf16[1,128,128]{2,1,0:T(8,128)(2,1)}, u32[]{:S(2)}) copy-start(bf16[1,128,128]{2,1,0:T(8,128)(2,1)} %param.32) | copy-start | bytes 98308

commit v2 on v1

--- a/solution.py
+++ b/solution.py
@@ -51,20 +51,23 @@
 
 
 def kernel(
-    x_ref, w_ref, r_ref, gate_ref, step_ref, extra_ref, lane_ref, bypass_ref,
-    xtap_ref, wtap_ref, rtap_ref, gain_ref, q_ref, k_ref, v_ref, g_ref, w1_ref, w2_ref,
+    x_in, w_in, r_in, gate_in, step_in, extra_in, lane_in, bypass_in, xtap_in, wtap_in, rtap_in,
+    gain_in, q_in, k_in, v_in, g_in, w1_ref, w2_ref,
     out_ref,
+    x_ref, w_ref, r_ref, gate_ref, step_ref, extra_ref, lane_ref, bypass_ref, xtap_ref, wtap_ref, rtap_ref,
+    gain_ref, q_ref, k_ref, v_ref, g_ref,
     kv, qs, wide, hx, hw, hr, m_sc, acc_sc, msg, s1, tot, s2, pre, cumpre, back, carried,
-    xs_sc, ms_sc, rd_sc, ecum_sc, wbuf, give, take,
+    xs_sc, ms_sc, rd_sc, ecum_sc, wbuf, give, take, keep,
     kv1_send, kv1_recv, kv_send, kv_recv, s1_send, s1_recv, s2_send, s2_recv, s3_send, s3_recv,
-    w_send, w_recv, own_sem, halo_send, halo_recv, tp_send, tp_recv,
+    w_send, w_recv, own_sem, halo_send, halo_recv, tp_send, tp_recv, in_sem, ready,
 ):
     z, y = lax.axis_index("sp_0"), lax.axis_index("sp_1")
     fx, tp = lax.axis_index("fs"), lax.axis_index("tp")
     me = z * RING + y
     maj = (z, y)
     axis_of = ("sp_0", "sp_1")
-    after, before = lax.rem(me + 1, RING * RING), lax.rem(me + RING * RING - 1, RING * RING)
+    after = lax.rem(me + 1, RING * RING)
+    last = RING - 1
 
     def at_sp(i):
         return {"sp_0": i // RING, "sp_1": lax.rem(i, RING)}
@@ -80,14 +83,51 @@
     low = lane < HD
     sub8 = lax.broadcasted_iota(jnp.int32, (8, ROWS), 0)
 
+    ins = [
+        pltpu.make_async_copy(src, dst, in_sem.at[i])
+        for i, (src, dst) in enumerate((
+            (k_in, k_ref), (v_in, v_ref), (g_in, g_ref), (q_in, q_ref), (x_in, x_ref), (w_in, w_ref),
+            (r_in, r_ref), (step_in, step_ref), (extra_in, extra_ref), (lane_in, lane_ref),
+            (bypass_in, bypass_ref), (xtap_in, xtap_ref), (wtap_in, wtap_ref), (rtap_in, rtap_ref),
+            (gate_in, gate_ref), (gain_in, gain_ref),
+        ))
+    ]
+    for copy in ins:
+        copy.start()
+
+    def clear_row(row, carry):
+        kv[0, row] = jnp.zeros((RING, BLOCK, ROWS), BF16)
+        kv[1, y, row] = jnp.zeros((BLOCK, ROWS), BF16)
+        return carry
+
+    lax.fori_loop(z + 1, RING, clear_row, 0)
+
+    @pl.when(z < 4)
+    def _():
+        kv[1, mod8(y + 4), 4:8] = jnp.zeros((4, BLOCK, ROWS), BF16)
+
+    barrier = pltpu.get_barrier_semaphore()
+
+    def greet(peer):
+        pl.semaphore_signal(barrier, inc=1, device_id=peer, device_id_type=MESH)
+
+    for d in range(1, RING):
+        greet({"sp_1": mod8(y + d)})
+    for peer in ({"fs": mod4(fx + 1)}, {"fs": mod4(fx - 1)}, {"tp": 1 - tp}):
+        greet(peer)
+    for d in range(1, RING):
+        pl.when(z + d < RING)(lambda d=d: greet({"sp_0": z + d}))
+    pl.when((y == 0) & (z > 0))(lambda: greet(at_sp(me - 1)))
+
+    wide[...] = jnp.zeros_like(wide)
+    for copy in ins[0:4]:
+        copy.wait()
     kf, vf = k_ref[...].astype(F32), v_ref[...].astype(F32)
     both = (
         jnp.where(low, kf, pltpu.roll(vf, HD, 1)).astype(BF16),
         jnp.where(low, pltpu.roll(kf, HD, 1), vf).astype(BF16),
     )
-    wide[...] = jnp.zeros_like(wide)
-    wide[:, 0:8] = g_ref[...]
-    gt = wide[...].T[0:8]
+    gt = g_ref[...]
     hi, mid, lo = split3(gt)
     four = sub8 < 4
     rows0 = jnp.concatenate(
@@ -105,36 +145,40 @@
         qs[2 * p] = jnp.where(low, qf, 0.0).astype(BF16)
         qs[2 * p + 1] = jnp.where(low, pltpu.roll(qf, HD, 1), 0.0).astype(BF16)
 
-    barrier = pltpu.get_barrier_semaphore()
-    peers = [{"sp_1": mod8(y + d)} for d in range(1, RING)]
-    peers += [{"sp_0": mod8(z + d)} for d in range(1, RING)]
-    peers += [{"fs": mod4(fx + 1)}, {"fs": mod4(fx - 1)}, {"tp": 1 - tp}]
-    peers += [at_sp(after), at_sp(before)]
-    for peer in peers:
-        pl.semaphore_signal(barrier, inc=1, device_id=peer, device_id_type=MESH)
-    pl.semaphore_wait(barrier, len(peers))
+    for copy in ins[4:7]:
+        copy.wait()
+    inner_row = (y < last) | (z == last)
+    pl.semaphore_wait(barrier, RING + 2 + z + jnp.where(inner_row, 0, 1))
+    for d in range(1, RING):
+        @pl.when(z - d >= 0)
+        def _():
+            pl.semaphore_signal(
+                ready.at[z], inc=1, device_id={"sp_0": z - d}, device_id_type=MESH
+            )
 
     halos = []
     for i, (src, dst) in enumerate(((x_ref, hx), (w_ref, hw), (r_ref, hr))):
         halos.append(
             remote(src.at[pl.ds(ROWS - 16, 16)], dst, halo_send.at[i], halo_recv.at[i], at_sp(after))
         )
-        halos[-1].start()
+
+    def each_halo(do):
+        for h in halos:
+            do(h)
+
+    pl.when(me < RING * RING - 1)(lambda: each_halo(lambda h: h.start()))
 
     def first(c, d):
-        peer = mod8(maj[1 - c] + d)
+        peer = mod8(y + d) if c == 0 else z + d
         own = kv.at[c, maj[c], maj[1 - c]]
-        return remote(own, own, kv1_send.at[c, d], kv1_recv.at[c, RING - d],
-                      {axis_of[1 - c]: peer})
-
-    def first_arrival(c, d):
-        peer = mod8(maj[1 - c] + d)
-        slot = kv.at[c, maj[c], peer]
-        return remote(slot, slot, kv1_send.at[c, d], kv1_recv.at[c, d], {axis_of[1 - c]: peer})
+        return remote(own, own, kv1_send.at[c, d], kv1_recv.at[c, maj[1 - c]], {axis_of[1 - c]: peer})
+
+    def first_arrival(c, b):
+        slot = kv.at[c, maj[c], b]
+        return remote(slot, slot, kv1_send.at[c, 0], kv1_recv.at[c, b], {axis_of[1 - c]: b})
 
     for d in range(1, RING):
-        for c in range(2):
-            first(c, d).start()
+        first(0, d).start()
 
     right, left = {"fs": mod4(fx + 1)}, {"fs": mod4(fx - 1)}
     owns = [
@@ -163,6 +207,12 @@
     for j in range(2):
         for d in range(2):
             weights(j, d).start()
+
+    for d in range(1, RING):
+        @pl.when(z + d < RING)
+        def _():
+            pl.semaphore_wait(ready.at[z + d], 1)
+            first(1, d).start()
 
     for h in range(8):
         c = h // 4
@@ -174,8 +224,13 @@
         m_sc[h] = jnp.broadcast_to(m, (ROWS, ROWS))
         acc_sc[h] = dot(p.astype(BF16), jnp.where(low, 1.0, own.astype(F32)).astype(BF16))
 
-    for h in halos:
-        h.wait_recv()
+    for copy in ins[7:]:
+        copy.wait()
+
+    @pl.when(me > 0)
+    def _():
+        each_halo(lambda h: h.wait_recv())
+
     opening = me > 0
 
     def filtered(rows, halo, taps):
@@ -193,9 +248,8 @@
     rd_sc[...] = rd
     raw = step_ref[...]
     step = jnp.maximum(raw, 0.0) + jnp.log1p(jnp.exp(-jnp.abs(raw)))
-    rate = jnp.zeros((8, ROWS), F32)
-    for h in range(8):
-        rate = jnp.where(sub8 == h, lane_ref[h], rate)
+    on_diagonal = sub8[:, 0:8] == lax.broadcasted_iota(jnp.int32, (8, 8), 1)
+    rate = jnp.sum(jnp.where(on_diagonal, lane_ref[...], 0.0), axis=1, keepdims=True)
     cum = step * (-jnp.exp(rate)) + extra_ref[...]
     lane8 = lax.broadcasted_iota(jnp.int32, (8, ROWS), 1)
     for shift in (1, 2, 4, 8, 16, 32, 64):
@@ -217,7 +271,7 @@
             mix = inner * (jnp.exp(gap) * step[h : h + 1, :])
             parts.append(dot(mix.astype(BF16), xp))
         xf = xp.astype(F32)
-        skip = jnp.where(low, bypass_ref[2 * p], bypass_ref[2 * p + 1])
+        skip = jnp.where(low, bypass_ref[:, 2 * p : 2 * p + 1], bypass_ref[:, 2 * p + 1 : 2 * p + 2])
         ms_sc[:, 128 * p : 128 * p + 128] = jnp.where(low, parts[0], parts[1]) + skip * xf
         ends = jnp.where(low, turned[:, 8 + 2 * p : 9 + 2 * p], turned[:, 9 + 2 * p : 10 + 2 * p])
         ecum_sc[:, 128 * p : 128 * p + 128] = jnp.exp(
@@ -250,6 +304,9 @@
         slot = dst.at[peer]
         return remote(slot, slot, send.at[d], recv.at[d], {axis: peer})
 
+    def up_total(d):
+        return remote(tot, s2.at[z], s2_send.at[d], s2_recv.at[z], {"sp_0": z + d})
+
     s1_out = [around(lambda p: msg.at[p], s1, s1_send, s1_recv, "sp_1", d) for d in range(1, RING)]
     for o in s1_out:
         o.start()
@@ -271,6 +328,25 @@
         slot = bundle(c, mod8(maj[c] + away), half)
         to = mod8(maj[c] + (1 if d == 0 else -1))
         return remote(slot, slot, kv_send.at[c, d, k], kv_recv.at[c, d, k], {axis_of[c]: to})
+
+    def going(c, d, k):
+        half = (0 if d == 0 else 1) if k == 6 else k % 2
+        if c == 1:
+            return z >= 4 * half
+        if d == 0:
+            return (z - k // 2 >= 0) & (z < last)
+        return mod8(z + k // 2) <= 2 + half
+
+    def coming(c, d, k):
+        half = (0 if d == 0 else 1) if k == 6 else k % 2
+        if c == 1:
+            return z >= 4 * half
+        if d == 0:
+            return z - 1 - k // 2 >= 0
+        return mod8(z + 1 + k // 2) <= 2 + half
+
+    def send(c, d, k):
+        pl.when(going(c, d, k))(lambda: hop(c, d, k).start())
 
     def attend(up, down, half_up, half_down):
         def one(c, carry):
@@ -310,17 +386,17 @@
 
         lax.fori_loop(0, 2, one, 0)
 
-    for d in range(1, RING):
+    for half in range(2):
         for c in range(2):
-            first_arrival(c, d).wait_recv()
-    for k in range(2):
-        for c in range(2):
+            for b in range(4 * half, 4 * half + 4):
+                there = (b != y) if c == 0 else (b < z)
+                pl.when(there)(lambda: first_arrival(c, b).wait_recv())
             for d in range(2):
-                hop(c, d, k).start()
+                send(c, d, half)
     attend(0, 0, 0, 1)
 
     def stage(k):
-        if k == 0:
+        if k == 2:
             weights_arrival(0, 0).wait_recv()
             passed_on(0).start()
         if k == 1:
@@ -337,11 +413,12 @@
             tot[0:HD] = run.astype(BF16)
             tot[HD:MSG] = decay_rows(jnp.broadcast_to(total, (8, ROWS)))
             for d in range(1, RING):
-                around(lambda p: tot, s2, s2_send, s2_recv, "sp_0", d).start()
+                pl.when(z + d < RING)(lambda: up_total(d).start())
         if k == 3:
-            for d in range(1, RING):
-                around_arrival(s2, s2_send, s2_recv, "sp_0", d).wait_recv()
-            s2[z] = tot[...]
+            for j in range(RING - 1):
+                slot = s2.at[j]
+                come = remote(slot, slot, s2_send.at[0], s2_recv.at[j], {"sp_0": j})
+                pl.when(j < z)(lambda: come.wait_recv())
             entering = jnp.zeros((HD, ROWS), F32)
             for j in range(RING - 1):
                 later = jnp.exp(decay_of(s2[j, HD:MSG])) * entering + s2[j, 0:HD].astype(F32)
@@ -351,10 +428,10 @@
             for d in range(1, RING):
                 around(lambda p: back.at[p], carried, s3_send, s3_recv, "sp_1", d).start()
             carried[y] = back[y]
-        if k == 4:
+        if k == 5:
             weights_arrival(1, 1).wait_recv()
             passed_on(1).start()
-        if k == 5:
+        if k == 6:
             for d in range(1, RING):
                 around_arrival(carried, s3_send, s3_recv, "sp_1", d).wait_recv()
             states = jnp.concatenate([carried[h] for h in range(8)], axis=0)
@@ -366,14 +443,14 @@
     for k in range(7):
         for c in range(2):
             for d in range(2):
-                hop_arrival(c, d, k).wait_recv()
+                pl.when(coming(c, d, k))(lambda: hop_arrival(c, d, k).wait_recv())
         for c in range(2):
             if k < 5:
-                hop(c, 0, k + 2).start()
+                send(c, 0, k + 2)
             if k < 4:
-                hop(c, 1, k + 2).start()
+                send(c, 1, k + 2)
             if k == 5:
-                hop(c, 1, 6).start()
+                send(c, 1, 6)
         half_up = 0 if k == 6 else k % 2
         half_down = 1 if k == 6 else k % 2
         attend(-(k // 2) - 1, k // 2 + 1, half_up, half_down)
@@ -387,40 +464,48 @@
         attended.append(jnp.where(low, first_half, second_half).astype(BF16))
     attended = jnp.concatenate(attended, axis=1)
     state_out = xs_sc[...]
-    for o in owns:
-        o.wait()
-    weights_arrival(0, 1).wait_recv()
-    weights_arrival(1, 0).wait_recv()
-    for j in range(2):
-        passed_arrival(j).wait_recv()
-    whole = []
     half_rows = ROWS // 2
-    for f in range(FS):
+
+    def across(n):
+        return remote(give.at[n], take.at[n], tp_send.at[n], tp_recv.at[n], {"tp": 1 - tp})
+
+    columns = (fx, mod4(fx - 1), mod4(fx + 1), mod4(fx + 2))
+    for n, f in enumerate(columns):
+        if n == 0:
+            for o in owns:
+                o.wait()
+        elif n == 1:
+            weights_arrival(1, 0).wait_recv()
+        elif n == 2:
+            weights_arrival(0, 1).wait_recv()
+        else:
+            passed_arrival(0).wait_recv()
+            passed_arrival(1).wait_recv()
         merged = dot(state_out, wbuf[0, f]) + dot(attended, wbuf[1, f])
         top, bottom = merged[0:half_rows], merged[half_rows:ROWS]
-        give[f] = jnp.where(tp == 0, bottom, top).astype(BF16)
-        copy = remote(give.at[f], take.at[f], tp_send.at[f], tp_recv.at[f], {"tp": 1 - tp})
-        copy.start()
-        whole.append(jnp.where(tp == 0, top, bottom))
-    for f in range(FS):
-        copy = remote(give.at[f], take.at[f], tp_send.at[f], tp_recv.at[f], {"tp": 1 - tp})
-        copy.wait_recv()
-        out_ref[:, 512 * f : 512 * f + 512] = (whole[f] + take[f].astype(F32)).astype(BF16)
-
-    for f in range(FS):
-        remote(give.at[f], take.at[f], tp_send.at[f], tp_recv.at[f], {"tp": 1 - tp}).wait_send()
-    for h in halos:
-        h.wait_send()
+        give[n] = jnp.where(tp == 0, bottom, top).astype(BF16)
+        across(n).start()
+        keep[n] = jnp.where(tp == 0, top, bottom)
+    for n, f in enumerate(columns):
+        across(n).wait_recv()
+        out_ref[:, pl.ds(pl.multiple_of(512 * f, 512), 512)] = (keep[n] + take[n].astype(F32)).astype(BF16)
+
+    for n in range(FS):
+        across(n).wait_send()
+    pl.when(me < RING * RING - 1)(lambda: each_halo(lambda h: h.wait_send()))
     for d in range(1, RING):
-        for c in range(2):
-            first(c, d).wait_send()
+        first(0, d).wait_send()
         around(lambda p: msg.at[p], s1, s1_send, s1_recv, "sp_1", d).wait_send()
-        around(lambda p: tot, s2, s2_send, s2_recv, "sp_0", d).wait_send()
         around(lambda p: back.at[p], carried, s3_send, s3_recv, "sp_1", d).wait_send()
+
+        @pl.when(z + d < RING)
+        def _():
+            first(1, d).wait_send()
+            up_total(d).wait_send()
     for k in range(7):
         for c in range(2):
             for d in range(2):
-                hop(c, d, k).wait_send()
+                pl.when(going(c, d, k))(lambda: hop(c, d, k).wait_send())
     for j in range(2):
         for d in range(2):
             weights(j, d).wait_send()
@@ -435,15 +520,20 @@
     state_out_weight, attention_out_weight,
 ):
     vmem = pl.BlockSpec(memory_space=pltpu.VMEM)
-    smem = pl.BlockSpec(memory_space=pltpu.SMEM)
-    anyw = pl.BlockSpec(memory_space=pl.ANY)
+    hbm = pl.BlockSpec(memory_space=pltpu.HBM)
     dma = pltpu.SemaphoreType.DMA
     out = pl.pallas_call(
         kernel,
         out_shape=jax.ShapeDtypeStruct((ROWS // 2, 512 * FS), BF16),
-        in_specs=[vmem] * 6 + [smem] * 2 + [vmem] * 8 + [anyw] * 2,
+        in_specs=[hbm] * 18,
         out_specs=vmem,
         scratch_shapes=[
+            pltpu.VMEM((ROWS, 512), BF16), pltpu.VMEM((ROWS, ROWS), BF16), pltpu.VMEM((ROWS, ROWS), BF16),
+            pltpu.VMEM((ROWS, 512), BF16), pltpu.VMEM((8, ROWS), F32), pltpu.VMEM((8, ROWS), F32),
+            pltpu.VMEM((1, 8), F32), pltpu.VMEM((1, 8), F32),
+            pltpu.VMEM((4, 512), BF16), pltpu.VMEM((4, ROWS), BF16), pltpu.VMEM((4, ROWS), BF16),
+            pltpu.VMEM((1, 512), F32), pltpu.VMEM((ROWS, 512), BF16), pltpu.VMEM((ROWS, ROWS), BF16),
+            pltpu.VMEM((ROWS, ROWS), BF16), pltpu.VMEM((8, ROWS), F32),
             pltpu.VMEM((2, RING, RING, BLOCK, ROWS), BF16),
             pltpu.VMEM((8, ROWS, ROWS), BF16),
             pltpu.VMEM((ROWS, ROWS), F32),
@@ -467,22 +557,25 @@
             pltpu.VMEM((2, FS, 512, 512), BF16),
             pltpu.VMEM((FS, ROWS // 2, 512), BF16),
             pltpu.VMEM((FS, ROWS // 2, 512), BF16),
+            pltpu.VMEM((FS, ROWS // 2, 512), F32),
             dma((2, RING)), dma((2, RING)),
             dma((2, 2, 7)), dma((2, 2, 7)),
             dma((RING,)), dma((RING,)), dma((RING,)), dma((RING,)), dma((RING,)), dma((RING,)),
             dma((2, 3)), dma((2, 3)), dma((2,)),
-            dma((3,)), dma((3,)), dma((FS,)), dma((FS,)),
+            dma((3,)), dma((3,)), dma((FS,)), dma((FS,)), dma((16,)),
+            pltpu.SemaphoreType.REGULAR((RING,)),
         ],
         compiler_params=pltpu.CompilerParams(
-            collective_id=0, has_side_effects=True, vmem_limit_bytes=48 * 1024 * 1024
+            collective_id=0, has_side_effects=True, vmem_limit_bytes=60 * 1024 * 1024
         ),
         name="mixer",
     )(
         state_head_inputs[0], state_write_vectors[0], state_read_vectors[0], state_output_gate[0],
-        presoftplus_steps[0], extra_decay_log[0], lane_shrinkage_powers, bypass_coefficient_vector,
+        presoftplus_steps[0], extra_decay_log[0],
+        lane_shrinkage_powers.reshape(1, -1), bypass_coefficient_vector.reshape(1, -1),
         feeder_smoothing_stencil, stored_smoothing_stencil, lookup_smoothing_stencil,
         bundled_rescaling_vector.reshape(1, -1), queries[0], attention_keys[0], attention_values[0],
-        forget_gate_cumsum[0], state_out_weight, attention_out_weight,
+        forget_gate_cumsum[0].T, state_out_weight, attention_out_weight,
     )
     return out[None]
 

time: 72.6 us -> 62.7 us (0.86)
  the two profiles are of different devices: /device:TPU:59 before, /device:TPU:315 now
where the time goes in v2:
time: 62.7 us; the launch traced here: 62.6 us
  Pallas kernels  60.9 us (97%)
  local copies, waits for them, and re-layouts  1.67 us (3%)
    pallas_call x1, Pallas kernels, shards(): pl.pallas_call(kernel, out_shape=jax.ShapeDtypeStruct((ROWS // 2, 512 * F...  60.9 us
    unnamed x1, local copies, waits for them, and re-layouts  1.67 us

profile of v2, /device:TPU:315, one launch (start us, length us, event | category | flops | bytes accessed | tf_op | source)
XLA Modules:
  0.0 62.6 jit_solution(8707129792536481051)
XLA Ops:
  0.0 60.9 %mixer.1 = bf16[64,2048]{1,0:T(8,128)(2,1)} custom-call(bf16[128,512]{1,0:T(8,128)(2,1)} %bitcast.17, bf16[128,128]{1,0:T(8,128)(2,1)} %bitcast.20, bf16[128,128]{1,0:T(8,128)(2,1)} %bitcast.21, bf16[128,512]{1,0:T(8,128)(2,1)} %bitcast.18, f32[8,128]{1,0:T(8,128)} %bitcast.24, f32[8,128]{1,0:T(8,128)} %bitcast.25, f32[1,8]{1,0:T(1,128)} %bitcast.28, ...), custom_call_target="tpu_custom_call" | custom-call | tf_op jit(solution)/shard_map/mixer/pallas_call | solution.py:525
  60.9 1.7 %copy.20 = bf16[1,64,2048]{2,1,0:T(8,128)(2,1)} copy(bf16[1,64,2048]{2,1,0:T(8,128)(2,1)} %bitcast.16) | data formatting | bytes 524288

commit v3 on v2

--- a/solution.py
+++ b/solution.py
@@ -122,28 +122,39 @@
     wide[...] = jnp.zeros_like(wide)
     for copy in ins[0:4]:
         copy.wait()
-    kf, vf = k_ref[...].astype(F32), v_ref[...].astype(F32)
-    both = (
-        jnp.where(low, kf, pltpu.roll(vf, HD, 1)).astype(BF16),
-        jnp.where(low, pltpu.roll(kf, HD, 1), vf).astype(BF16),
+    kf, vt = k_ref[...].astype(F32), v_ref[...].astype(F32).T
+    low64 = low[0:HD]
+    key_rows = (
+        jnp.where(low64, kf[0:HD], pltpu.roll(kf[HD:ROWS], HD, 1)),
+        jnp.where(low64, pltpu.roll(kf[0:HD], HD, 1), kf[HD:ROWS]),
     )
-    gt = g_ref[...]
-    hi, mid, lo = split3(gt)
+    hi, mid, lo = split3(-g_ref[...])
     four = sub8 < 4
-    rows0 = jnp.concatenate(
-        [jnp.where(four, hi, pltpu.roll(lo, 4, 0)), jnp.where(four, mid, 0.0)], axis=0
+    gate_rows = (
+        jnp.concatenate(
+            [jnp.where(four, hi, pltpu.roll(lo, 4, 0)), jnp.where(four, mid, 0.0)], axis=0
+        ),
+        jnp.concatenate(
+            [jnp.where(four, pltpu.roll(hi, 4, 0), lo), jnp.where(four, pltpu.roll(mid, 4, 0), 0.0)],
+            axis=0,
+        ),
     )
-    rows1 = jnp.concatenate(
-        [jnp.where(four, pltpu.roll(hi, 4, 0), lo), jnp.where(four, pltpu.roll(mid, 4, 0), 0.0)], axis=0
-    )
-    kv[0, z, y, 0:ROWS] = both[0]
-    kv[1, y, z, 0:ROWS] = both[1]
-    kv[0, z, y, ROWS:BLOCK] = rows0.astype(BF16)
-    kv[1, y, z, ROWS:BLOCK] = rows1.astype(BF16)
-    for p in range(4):
+    for c in range(2):
+        spot = (c, maj[c], maj[1 - c])
+        kv[spot + (slice(0, HD),)] = key_rows[c].astype(BF16)
+        kv[spot + (slice(HD, ROWS),)] = vt[HD * c : HD * c + HD].astype(BF16)
+        kv[spot + (slice(ROWS, BLOCK),)] = gate_rows[c].astype(BF16)
+    for h in range(8):
+        p, e = h // 2, h % 2
         qf = q_ref[:, 128 * p : 128 * p + 128].astype(F32) * 0.125
-        qs[2 * p] = jnp.where(low, qf, 0.0).astype(BF16)
-        qs[2 * p + 1] = jnp.where(low, pltpu.roll(qf, HD, 1), 0.0).astype(BF16)
+        turn = pltpu.roll(qf, HD, 1)
+        at = slice(ROWS * e, ROWS * e + ROWS)
+        picks = jnp.where(lax.rem(lane, 4) == h % 4, 1.0, 0.0).astype(BF16)
+        head, other = (qf, turn) if e == 0 else (turn, qf)
+        qs[p, 0, at, 0:ROWS] = jnp.where(low, head, 0.0).astype(BF16)
+        qs[p, 1, at, 0:ROWS] = jnp.where(low, 0.0, other).astype(BF16)
+        for n in range(2):
+            qs[p, n, at, ROWS : 2 * ROWS] = picks
 
     for copy in ins[4:7]:
         copy.wait()
@@ -214,15 +225,33 @@
             pl.semaphore_wait(ready.at[z + d], 1)
             first(1, d).start()
 
-    for h in range(8):
-        c = h // 4
-        own = both[c]
-        s = dot(qs[h], own, NT) - gt[h : h + 1, :]
-        s = jnp.where(lane <= sub, s, NEG)
-        m = jnp.max(s, axis=1, keepdims=True)
-        p = jnp.exp(s - m)
-        m_sc[h] = jnp.broadcast_to(m, (ROWS, ROWS))
-        acc_sc[h] = dot(p.astype(BF16), jnp.where(low, 1.0, own.astype(F32)).astype(BF16))
+    ones = jnp.ones((16, ROWS), BF16)
+    pair_query = lax.rem(lax.broadcasted_iota(jnp.int32, (HD, 2 * ROWS), 1), ROWS)
+    pair_key = lax.broadcasted_iota(jnp.int32, (HD, 2 * ROWS), 0)
+    lane_block = lane // 16
+
+    def turned_gates(gates):
+        f = jnp.concatenate([g.astype(F32) for g in gates], axis=0)
+        if f.shape[0] < ROWS:
+            f = jnp.concatenate([f, jnp.zeros((ROWS - f.shape[0], ROWS), F32)], axis=0)
+        return f.T
+
+    def scores(keys, gates, p, n):
+        return dot(jnp.concatenate([keys, gates], axis=1), qs[p, n], NT)
+
+    for c in range(2):
+        own = kv.at[c, maj[c], maj[1 - c]]
+        turned = turned_gates([own[ROWS:BLOCK]]).astype(BF16)
+        vals = jnp.concatenate([own[HD:ROWS], ones], axis=0)
+        for p in (2 * c, 2 * c + 1):
+            s0 = scores(own[0:HD], turned[0:HD], p, 0)
+            s1_ = scores(own[0:HD], turned[HD:ROWS], p, 1)
+            s0 = jnp.where(pair_key <= pair_query, s0, NEG)
+            s1_ = jnp.where(pair_key + HD <= pair_query, s1_, NEG)
+            m = jnp.maximum(jnp.max(s0, axis=0, keepdims=True), jnp.max(s1_, axis=0, keepdims=True))
+            probs = jnp.concatenate([jnp.exp(s0 - m), jnp.exp(s1_ - m)], axis=0).astype(BF16)
+            m_sc[p] = jnp.broadcast_to(m, (8, 2 * ROWS))
+            acc_sc[p] = dot(vals, probs)
 
     for copy in ins[7:]:
         copy.wait()
@@ -359,28 +388,38 @@
 
             @pl.when(jnp.minimum(lead_u, lead_d) < me)
             def _():
-                keys, bias, vals = [], [], []
-                for row, half, lead in ((row_u, half_up, lead_u), (row_d, half_down, lead_d)):
-                    for b in range(4):
-                        rows = kv[c, row, 4 * half + b, 0:ROWS]
-                        g = kv[c, row, 4 * half + b, ROWS:BLOCK].astype(F32)
-                        g = g[0:8] + g[8:16]
-                        g = g + pltpu.roll(g, 4, 0)
-                        seen = lead + b * inner_stride < me
-                        bias.append(jnp.where(seen, -g, NEG))
-                        keys.append(rows)
-                        vals.append(jnp.where(low, jnp.ones_like(rows), rows))
-                keys = jnp.concatenate(keys, axis=0)
-                vals = jnp.concatenate(vals, axis=0)
-                bias = jnp.concatenate(bias, axis=1)
-                for i in range(4):
-                    h = 4 * c + i
-                    s = dot(qs[h], keys, NT) + bias[i : i + 1, :]
-                    m_old = m_sc[h]
-                    m_new = jnp.maximum(m_old, jnp.max(s, axis=1, keepdims=True))
-                    m_sc[h] = m_new
-                    p = jnp.exp(s - m_new[:, 0:1])
-                    acc_sc[h] = acc_sc[h] * jnp.exp(m_old - m_new) + dot(p.astype(BF16), vals)
+                spots = [(row_u, 4 * half_up + b) for b in range(4)]
+                spots += [(row_d, 4 * half_down + b) for b in range(4)]
+                leads = [lead_u + b * inner_stride for b in range(4)]
+                leads += [lead_d + b * inner_stride for b in range(4)]
+                turned = turned_gates([kv[c, r, b, ROWS:BLOCK] for r, b in spots])
+                gates = []
+                for n, lead in enumerate(leads):
+                    off = jnp.where(lead < me, 0.0, NEG)
+                    gates.append(jnp.where(lane_block == n, turned + off, 0.0).astype(BF16))
+                for part in range(2):
+                    at = range(4 * part, 4 * part + 4)
+                    keys = jnp.concatenate([kv[(c,) + spots[n] + (slice(0, HD),)] for n in at], axis=0)
+                    vals = [kv[(c,) + spots[n] + (slice(HD, ROWS),)] for n in at]
+                    vals = jnp.concatenate(
+                        [jnp.concatenate(vals, axis=1), jnp.concatenate([ones] * 4, axis=1)], axis=0
+                    )
+                    gates_0 = jnp.concatenate([gates[n][0:HD] for n in at], axis=0)
+                    gates_1 = jnp.concatenate([gates[n][HD:ROWS] for n in at], axis=0)
+                    for i in range(2):
+                        p = 2 * c + i
+                        s0 = scores(keys, gates_0, p, 0)
+                        s1_ = scores(keys, gates_1, p, 1)
+                        m_old = m_sc[p, 0:1]
+                        m = jnp.max(jnp.maximum(s0, s1_), axis=0, keepdims=True)
+                        m = jnp.maximum(m, m_old)
+                        m_sc[p, 0:1] = m
+                        e0, e1 = jnp.exp(s0 - m).astype(BF16), jnp.exp(s1_ - m).astype(BF16)
+                        probs = []
+                        for b in range(4):
+                            probs += [e0[HD * b : HD * b + HD], e1[HD * b : HD * b + HD]]
+                        probs = jnp.concatenate(probs, axis=0)
+                        acc_sc[p] = acc_sc[p] * jnp.exp(m_old - m) + dot(vals, probs)
 
             return carry
 
@@ -458,10 +497,10 @@
 
     attended = []
     for p in range(4):
-        a, b = acc_sc[2 * p], acc_sc[2 * p + 1]
-        first_half = pltpu.roll(a, HD, 1) / a
-        second_half = b / pltpu.roll(b, HD, 1)
-        attended.append(jnp.where(low, first_half, second_half).astype(BF16))
+        acc = acc_sc[p]
+        out = acc[0:HD] / acc[HD : HD + 1]
+        out = jnp.concatenate([out[:, 0:ROWS], out[:, ROWS : 2 * ROWS]], axis=0)
+        attended.append(out.T.astype(BF16))
     attended = jnp.concatenate(attended, axis=1)
     state_out = xs_sc[...]
     half_rows = ROWS // 2
@@ -535,13 +574,13 @@
             pltpu.VMEM((1, 512), F32), pltpu.VMEM((ROWS, 512), BF16), pltpu.VMEM((ROWS, ROWS), BF16),
             pltpu.VMEM((ROWS, ROWS), BF16), pltpu.VMEM((8, ROWS), F32),
             pltpu.VMEM((2, RING, RING, BLOCK, ROWS), BF16),
-            pltpu.VMEM((8, ROWS, ROWS), BF16),
+            pltpu.VMEM((4, 2, 2 * ROWS, 2 * ROWS), BF16),
             pltpu.VMEM((ROWS, ROWS), F32),
             pltpu.VMEM((16, 512), BF16),
             pltpu.VMEM((16, ROWS), BF16),
             pltpu.VMEM((16, ROWS), BF16),
-            pltpu.VMEM((8, ROWS, ROWS), F32),
-            pltpu.VMEM((8, ROWS, ROWS), F32),
+            pltpu.VMEM((4, 8, 2 * ROWS), F32),
+            pltpu.VMEM((4, HD + 16, 2 * ROWS), F32),
             pltpu.VMEM((RING, MSG, ROWS), BF16),
             pltpu.VMEM((RING, MSG, ROWS), BF16),
             pltpu.VMEM((MSG, ROWS), BF16),

time: 62.7 us -> 60.2 us (0.960)
  the two profiles are of different devices: /device:TPU:315 before, /device:TPU:195 now
where the time goes in v3:
time: 60.2 us; the launch traced here: 60 us
  Pallas kernels  58.3 us (97%)
  local copies, waits for them, and re-layouts  1.67 us (3%)
    pallas_call x1, Pallas kernels, shards(): pl.pallas_call(kernel, out_shape=jax.ShapeDtypeStruct((ROWS // 2, 512 * F...  58.3 us
    unnamed x1, local copies, waits for them, and re-layouts  1.67 us

profile of v3, /device:TPU:195, one launch (start us, length us, event | category | flops | bytes accessed | tf_op | source)
XLA Modules:
  0.0 60.0 jit_solution(423072099172403345)
XLA Ops:
  0.0 58.3 %mixer.1 = bf16[64,2048]{1,0:T(8,128)(2,1)} custom-call(bf16[128,512]{1,0:T(8,128)(2,1)} %bitcast.17, bf16[128,128]{1,0:T(8,128)(2,1)} %bitcast.20, bf16[128,128]{1,0:T(8,128)(2,1)} %bitcast.21, bf16[128,512]{1,0:T(8,128)(2,1)} %bitcast.18, f32[8,128]{1,0:T(8,128)} %bitcast.24, f32[8,128]{1,0:T(8,128)} %bitcast.25, f32[1,8]{1,0:T(1,128)} %bitcast.28, ...), custom_call_target="tpu_custom_call" | custom-call | tf_op jit(solution)/shard_map/mixer/pallas_call | solution.py:564
  58.3 1.7 %copy.20 = bf16[1,64,2048]{2,1,0:T(8,128)(2,1)} copy(bf16[1,64,2048]{2,1,0:T(8,128)(2,1)} %bitcast.16) | data formatting | bytes 524288

commit v4 on v3

--- a/solution.py
+++ b/solution.py
@@ -57,9 +57,9 @@
     x_ref, w_ref, r_ref, gate_ref, step_ref, extra_ref, lane_ref, bypass_ref, xtap_ref, wtap_ref, rtap_ref,
     gain_ref, q_ref, k_ref, v_ref, g_ref,
     kv, qs, wide, hx, hw, hr, m_sc, acc_sc, msg, s1, tot, s2, pre, cumpre, back, carried,
-    xs_sc, ms_sc, rd_sc, ecum_sc, wbuf, give, take, keep,
+    xs_sc, ms_sc, rd_sc, ecum_sc, wbuf, give, take, keep, ob,
     kv1_send, kv1_recv, kv_send, kv_recv, s1_send, s1_recv, s2_send, s2_recv, s3_send, s3_recv,
-    w_send, w_recv, own_sem, halo_send, halo_recv, tp_send, tp_recv, in_sem, ready,
+    w_send, w_recv, own_sem, halo_send, halo_recv, tp_send, tp_recv, in_sem, out_sem, ready, ready_row,
 ):
     z, y = lax.axis_index("sp_0"), lax.axis_index("sp_1")
     fx, tp = lax.axis_index("fs"), lax.axis_index("tp")
@@ -111,12 +111,11 @@
     def greet(peer):
         pl.semaphore_signal(barrier, inc=1, device_id=peer, device_id_type=MESH)
 
-    for d in range(1, RING):
-        greet({"sp_1": mod8(y + d)})
     for peer in ({"fs": mod4(fx + 1)}, {"fs": mod4(fx - 1)}, {"tp": 1 - tp}):
         greet(peer)
     for d in range(1, RING):
         pl.when(z + d < RING)(lambda d=d: greet({"sp_0": z + d}))
+        pl.when(y + d < RING)(lambda d=d: greet({"sp_1": y + d}))
     pl.when((y == 0) & (z > 0))(lambda: greet(at_sp(me - 1)))
 
     wide[...] = jnp.zeros_like(wide)
@@ -159,7 +158,7 @@
     for copy in ins[4:7]:
         copy.wait()
     inner_row = (y < last) | (z == last)
-    pl.semaphore_wait(barrier, RING + 2 + z + jnp.where(inner_row, 0, 1))
+    pl.semaphore_wait(barrier, 3 + z + y + jnp.where(inner_row, 0, 1))
     for d in range(1, RING):
         @pl.when(z - d >= 0)
         def _():
@@ -167,6 +166,42 @@
                 ready.at[z], inc=1, device_id={"sp_0": z - d}, device_id_type=MESH
             )
 
+        @pl.when(y - d >= 0)
+        def _():
+            pl.semaphore_signal(
+                ready_row.at[y], inc=1, device_id={"sp_1": y - d}, device_id_type=MESH
+            )
+
+    right, left = {"fs": mod4(fx + 1)}, {"fs": mod4(fx - 1)}
+    owns = [
+        pltpu.make_async_copy(w1_ref, wbuf.at[0, fx], own_sem.at[0]),
+        pltpu.make_async_copy(w2_ref, wbuf.at[1, fx], own_sem.at[1]),
+    ]
+
+    def weights(j, d):
+        src = (w1_ref, w2_ref)[j]
+        return remote(src, wbuf.at[j, fx], w_send.at[j, d], w_recv.at[j, d], (right, left)[d])
+
+    def weights_arrival(j, d):
+        slot = wbuf.at[j, mod4(fx - 1) if d == 0 else mod4(fx + 1)]
+        return remote(slot, slot, w_send.at[j, d], w_recv.at[j, d], (right, left)[d])
+
+    def passed_on(j):
+        slot = wbuf.at[j, mod4(fx - 1) if j == 0 else mod4(fx + 1)]
+        return remote(slot, slot, w_send.at[j, 2], w_recv.at[j, 2], (right, left)[j])
+
+    def passed_arrival(j):
+        slot = wbuf.at[j, mod4(fx + 2)]
+        return remote(slot, slot, w_send.at[j, 2], w_recv.at[j, 2], (right, left)[j])
+
+    for o in owns:
+        o.start()
+    for j, d in ((0, 0), (1, 1), (1, 0), (0, 1)):
+        weights(j, d).start()
+
+    for d in range(1, RING):
+        pl.when(y + d < RING)(lambda: pl.semaphore_wait(ready_row.at[y + d], 1))
+
     halos = []
     for i, (src, dst) in enumerate(((x_ref, hx), (w_ref, hw), (r_ref, hr))):
         halos.append(
@@ -190,34 +225,6 @@
 
     for d in range(1, RING):
         first(0, d).start()
-
-    right, left = {"fs": mod4(fx + 1)}, {"fs": mod4(fx - 1)}
-    owns = [
-        pltpu.make_async_copy(w1_ref, wbuf.at[0, fx], own_sem.at[0]),
-        pltpu.make_async_copy(w2_ref, wbuf.at[1, fx], own_sem.at[1]),
-    ]
-
-    def weights(j, d):
-        src = (w1_ref, w2_ref)[j]
-        return remote(src, wbuf.at[j, fx], w_send.at[j, d], w_recv.at[j, d], (right, left)[d])
-
-    def weights_arrival(j, d):
-        slot = wbuf.at[j, mod4(fx - 1) if d == 0 else mod4(fx + 1)]
-        return remote(slot, slot, w_send.at[j, d], w_recv.at[j, d], (right, left)[d])
-
-    def passed_on(j):
-        slot = wbuf.at[j, mod4(fx - 1) if j == 0 else mod4(fx + 1)]
-        return remote(slot, slot, w_send.at[j, 2], w_recv.at[j, 2], (right, left)[j])
-
-    def passed_arrival(j):
-        slot = wbuf.at[j, mod4(fx + 2)]
-        return remote(slot, slot, w_send.at[j, 2], w_recv.at[j, 2], (right, left)[j])
-
-    for o in owns:
-        o.start()
-    for j in range(2):
-        for d in range(2):
-            weights(j, d).start()
 
     for d in range(1, RING):
         @pl.when(z + d < RING)
@@ -377,7 +384,7 @@
     def send(c, d, k):
         pl.when(going(c, d, k))(lambda: hop(c, d, k).start())
 
-    def attend(up, down, half_up, half_down):
+    def attend(head, up, down, half_up, half_down):
         def one(c, carry):
             mine = jnp.where(c == 0, z, y)
             row_u, row_d = mod8(mine + up), mod8(mine + down)
@@ -397,12 +404,12 @@
                 for n, lead in enumerate(leads):
                     off = jnp.where(lead < me, 0.0, NEG)
                     gates.append(jnp.where(lane_block == n, turned + off, 0.0).astype(BF16))
-                for part in range(2):
-                    at = range(4 * part, 4 * part + 4)
+                for part in range(1):
+                    at = range(8)
                     keys = jnp.concatenate([kv[(c,) + spots[n] + (slice(0, HD),)] for n in at], axis=0)
                     vals = [kv[(c,) + spots[n] + (slice(HD, ROWS),)] for n in at]
                     vals = jnp.concatenate(
-                        [jnp.concatenate(vals, axis=1), jnp.concatenate([ones] * 4, axis=1)], axis=0
+                        [jnp.concatenate(vals, axis=1), jnp.concatenate([ones] * len(at), axis=1)], axis=0
                     )
                     gates_0 = jnp.concatenate([gates[n][0:HD] for n in at], axis=0)
                     gates_1 = jnp.concatenate([gates[n][HD:ROWS] for n in at], axis=0)
@@ -416,29 +423,36 @@
                         m_sc[p, 0:1] = m
                         e0, e1 = jnp.exp(s0 - m).astype(BF16), jnp.exp(s1_ - m).astype(BF16)
                         probs = []
-                        for b in range(4):
+                        for b in range(len(at)):
                             probs += [e0[HD * b : HD * b + HD], e1[HD * b : HD * b + HD]]
                         probs = jnp.concatenate(probs, axis=0)
                         acc_sc[p] = acc_sc[p] * jnp.exp(m_old - m) + dot(vals, probs)
 
             return carry
 
-        lax.fori_loop(0, 2, one, 0)
-
-    for half in range(2):
-        for c in range(2):
-            for b in range(4 * half, 4 * half + 4):
-                there = (b != y) if c == 0 else (b < z)
-                pl.when(there)(lambda: first_arrival(c, b).wait_recv())
-            for d in range(2):
-                send(c, d, half)
-    attend(0, 0, 0, 1)
+        one(head, 0)
+
+    def arrive(c, half):
+        for b in range(4 * half, 4 * half + 4):
+            there = (b != y) if c == 0 else (b < z)
+            pl.when(there)(lambda: first_arrival(c, b).wait_recv())
+        for d in range(2):
+            send(c, d, half)
+
+    arrive(1, 0)
+    arrive(1, 1)
+    attend(1, 0, 0, 0, 1)
+    arrive(0, 0)
+    arrive(0, 1)
+    attend(0, 0, 0, 0, 1)
 
     def stage(k):
-        if k == 2:
+        if k == 0:
             weights_arrival(0, 0).wait_recv()
             passed_on(0).start()
-        if k == 1:
+            weights_arrival(1, 1).wait_recv()
+            passed_on(1).start()
+        if k == -1:
             for d in range(1, RING):
                 around_arrival(s1, s1_send, s1_recv, "sp_1", d).wait_recv()
             run = jnp.zeros((HD, ROWS), F32)
@@ -453,7 +467,7 @@
             tot[HD:MSG] = decay_rows(jnp.broadcast_to(total, (8, ROWS)))
             for d in range(1, RING):
                 pl.when(z + d < RING)(lambda: up_total(d).start())
-        if k == 3:
+        if k == 2:
             for j in range(RING - 1):
                 slot = s2.at[j]
                 come = remote(slot, slot, s2_send.at[0], s2_recv.at[j], {"sp_0": j})
@@ -468,9 +482,6 @@
                 around(lambda p: back.at[p], carried, s3_send, s3_recv, "sp_1", d).start()
             carried[y] = back[y]
         if k == 5:
-            weights_arrival(1, 1).wait_recv()
-            passed_on(1).start()
-        if k == 6:
             for d in range(1, RING):
                 around_arrival(carried, s3_send, s3_recv, "sp_1", d).wait_recv()
             states = jnp.concatenate([carried[h] for h in range(8)], axis=0)
@@ -479,20 +490,20 @@
             stretch = lax.rsqrt(jnp.mean(u * u, axis=1, keepdims=True) + EPSILON)
             xs_sc[...] = (u * stretch * gain_ref[...]).astype(BF16)
 
+    stage(-1)
     for k in range(7):
-        for c in range(2):
+        half_up = 0 if k == 6 else k % 2
+        half_down = 1 if k == 6 else k % 2
+        for c in (1, 0):
             for d in range(2):
                 pl.when(coming(c, d, k))(lambda: hop_arrival(c, d, k).wait_recv())
-        for c in range(2):
             if k < 5:
                 send(c, 0, k + 2)
             if k < 4:
                 send(c, 1, k + 2)
             if k == 5:
                 send(c, 1, 6)
-        half_up = 0 if k == 6 else k % 2
-        half_down = 1 if k == 6 else k % 2
-        attend(-(k // 2) - 1, k // 2 + 1, half_up, half_down)
+            attend(c, -(k // 2) - 1, k // 2 + 1, half_up, half_down)
         stage(k)
 
     attended = []
@@ -507,6 +518,11 @@
 
     def across(n):
         return remote(give.at[n], take.at[n], tp_send.at[n], tp_recv.at[n], {"tp": 1 - tp})
+
+    def written(n, f):
+        return pltpu.make_async_copy(
+            ob.at[n], out_ref.at[:, pl.ds(pl.multiple_of(512 * f, 512), 512)], out_sem.at[n]
+        )
 
     columns = (fx, mod4(fx - 1), mod4(fx + 1), mod4(fx + 2))
     for n, f in enumerate(columns):
@@ -527,7 +543,10 @@
         keep[n] = jnp.where(tp == 0, top, bottom)
     for n, f in enumerate(columns):
         across(n).wait_recv()
-        out_ref[:, pl.ds(pl.multiple_of(512 * f, 512), 512)] = (keep[n] + take[n].astype(F32)).astype(BF16)
+        ob[n] = (keep[n] + take[n].astype(F32)).astype(BF16)
+        written(n, f).start()
+    for n, f in enumerate(columns):
+        written(n, f).wait()
 
     for n in range(FS):
         across(n).wait_send()
@@ -558,14 +577,13 @@
     bundled_rescaling_vector, queries, attention_keys, attention_values, forget_gate_cumsum,
     state_out_weight, attention_out_weight,
 ):
-    vmem = pl.BlockSpec(memory_space=pltpu.VMEM)
     hbm = pl.BlockSpec(memory_space=pltpu.HBM)
     dma = pltpu.SemaphoreType.DMA
     out = pl.pallas_call(
         kernel,
         out_shape=jax.ShapeDtypeStruct((ROWS // 2, 512 * FS), BF16),
         in_specs=[hbm] * 18,
-        out_specs=vmem,
+        out_specs=hbm,
         scratch_shapes=[
             pltpu.VMEM((ROWS, 512), BF16), pltpu.VMEM((ROWS, ROWS), BF16), pltpu.VMEM((ROWS, ROWS), BF16),
             pltpu.VMEM((ROWS, 512), BF16), pltpu.VMEM((8, ROWS), F32), pltpu.VMEM((8, ROWS), F32),
@@ -597,12 +615,13 @@
             pltpu.VMEM((FS, ROWS // 2, 512), BF16),
             pltpu.VMEM((FS, ROWS // 2, 512), BF16),
             pltpu.VMEM((FS, ROWS // 2, 512), F32),
+            pltpu.VMEM((FS, ROWS // 2, 512), BF16),
             dma((2, RING)), dma((2, RING)),
             dma((2, 2, 7)), dma((2, 2, 7)),
             dma((RING,)), dma((RING,)), dma((RING,)), dma((RING,)), dma((RING,)), dma((RING,)),
             dma((2, 3)), dma((2, 3)), dma((2,)),
-            dma((3,)), dma((3,)), dma((FS,)), dma((FS,)), dma((16,)),
-            pltpu.SemaphoreType.REGULAR((RING,)),
+            dma((3,)), dma((3,)), dma((FS,)), dma((FS,)), dma((16,)), dma((FS,)),
+            pltpu.SemaphoreType.REGULAR((RING,)), pltpu.SemaphoreType.REGULAR((RING,)),
         ],
         compiler_params=pltpu.CompilerParams(
             collective_id=0, has_side_effects=True, vmem_limit_bytes=60 * 1024 * 1024

time: 60.2 us -> 57 us (0.947)
  the two profiles are of different devices: /device:TPU:195 before, /device:TPU:257 now
where the time goes in v4:
time: 57 us; the launch traced here: 56.9 us
  Pallas kernels  55.2 us (97%)
  local copies, waits for them, and re-layouts  1.67 us (3%)
    pallas_call x1, Pallas kernels, shards(): pl.pallas_call(kernel, out_shape=jax.ShapeDtypeStruct((ROWS // 2, 512 * F...  55.2 us
    unnamed x1, local copies, waits for them, and re-layouts  1.67 us

profile of v4, /device:TPU:257, one launch (start us, length us, event | category | flops | bytes accessed | tf_op | source)
XLA Modules:
  0.0 56.9 jit_solution(16242897810181734152)
XLA Ops:
  0.0 55.2 %mixer.1 = bf16[64,2048]{1,0:T(8,128)(2,1)} custom-call(bf16[128,512]{1,0:T(8,128)(2,1)} %bitcast.17, bf16[128,128]{1,0:T(8,128)(2,1)} %bitcast.20, bf16[128,128]{1,0:T(8,128)(2,1)} %bitcast.21, bf16[128,512]{1,0:T(8,128)(2,1)} %bitcast.18, f32[8,128]{1,0:T(8,128)} %bitcast.24, f32[8,128]{1,0:T(8,128)} %bitcast.25, f32[1,8]{1,0:T(1,128)} %bitcast.28, ...), custom_call_target="tpu_custom_call" | custom-call | tf_op jit(solution)/shard_map/mixer/pallas_call | solution.py:582
  55.2 1.7 %copy.20 = bf16[1,64,2048]{2,1,0:T(8,128)(2,1)} copy(bf16[1,64,2048]{2,1,0:T(8,128)(2,1)} %bitcast.16) | data formatting | bytes 524288

commit v5 on v4

--- a/solution.py
+++ b/solution.py
@@ -57,7 +57,7 @@
     x_ref, w_ref, r_ref, gate_ref, step_ref, extra_ref, lane_ref, bypass_ref, xtap_ref, wtap_ref, rtap_ref,
     gain_ref, q_ref, k_ref, v_ref, g_ref,
     kv, qs, wide, hx, hw, hr, m_sc, acc_sc, msg, s1, tot, s2, pre, cumpre, back, carried,
-    xs_sc, ms_sc, rd_sc, ecum_sc, wbuf, give, take, keep, ob,
+    xs_sc, ms_sc, rd_sc, ecum_sc, wbuf, give, take, keep, ob, early,
     kv1_send, kv1_recv, kv_send, kv_recv, s1_send, s1_recv, s2_send, s2_recv, s3_send, s3_recv,
     w_send, w_recv, own_sem, halo_send, halo_recv, tp_send, tp_recv, in_sem, out_sem, ready, ready_row,
 ):
@@ -117,6 +117,48 @@
         pl.when(z + d < RING)(lambda d=d: greet({"sp_0": z + d}))
         pl.when(y + d < RING)(lambda d=d: greet({"sp_1": y + d}))
     pl.when((y == 0) & (z > 0))(lambda: greet(at_sp(me - 1)))
+
+    inner_row = (y < last) | (z == last)
+    pl.semaphore_wait(barrier, 3 + z + y + jnp.where(inner_row, 0, 1))
+    for d in range(1, RING):
+        @pl.when(z - d >= 0)
+        def _():
+            pl.semaphore_signal(
+                ready.at[z], inc=1, device_id={"sp_0": z - d}, device_id_type=MESH
+            )
+
+        @pl.when(y - d >= 0)
+        def _():
+            pl.semaphore_signal(
+                ready_row.at[y], inc=1, device_id={"sp_1": y - d}, device_id_type=MESH
+            )
+
+    right, left = {"fs": mod4(fx + 1)}, {"fs": mod4(fx - 1)}
+    owns = [
+        pltpu.make_async_copy(w1_ref, wbuf.at[0, fx], own_sem.at[0]),
+        pltpu.make_async_copy(w2_ref, wbuf.at[1, fx], own_sem.at[1]),
+    ]
+
+    def weights(j, d):
+        src = (w1_ref, w2_ref)[j]
+        return remote(src, wbuf.at[j, fx], w_send.at[j, d], w_recv.at[j, d], (right, left)[d])
+
+    def weights_arrival(j, d):
+        slot = wbuf.at[j, mod4(fx - 1) if d == 0 else mod4(fx + 1)]
+        return remote(slot, slot, w_send.at[j, d], w_recv.at[j, d], (right, left)[d])
+
+    def passed_on(j):
+        slot = wbuf.at[j, mod4(fx - 1) if j == 0 else mod4(fx + 1)]
+        return remote(slot, slot, w_send.at[j, 2], w_recv.at[j, 2], (right, left)[j])
+
+    def passed_arrival(j):
+        slot = wbuf.at[j, mod4(fx + 2)]
+        return remote(slot, slot, w_send.at[j, 2], w_recv.at[j, 2], (right, left)[j])
+
+    for o in owns:
+        o.start()
+    for j, d in ((0, 0), (1, 1), (1, 0), (0, 1)):
+        weights(j, d).start()
 
     wide[...] = jnp.zeros_like(wide)
     for copy in ins[0:4]:
@@ -157,48 +199,6 @@
 
     for copy in ins[4:7]:
         copy.wait()
-    inner_row = (y < last) | (z == last)
-    pl.semaphore_wait(barrier, 3 + z + y + jnp.where(inner_row, 0, 1))
-    for d in range(1, RING):
-        @pl.when(z - d >= 0)
-        def _():
-            pl.semaphore_signal(
-                ready.at[z], inc=1, device_id={"sp_0": z - d}, device_id_type=MESH
-            )
-
-        @pl.when(y - d >= 0)
-        def _():
-            pl.semaphore_signal(
-                ready_row.at[y], inc=1, device_id={"sp_1": y - d}, device_id_type=MESH
-            )
-
-    right, left = {"fs": mod4(fx + 1)}, {"fs": mod4(fx - 1)}
-    owns = [
-        pltpu.make_async_copy(w1_ref, wbuf.at[0, fx], own_sem.at[0]),
-        pltpu.make_async_copy(w2_ref, wbuf.at[1, fx], own_sem.at[1]),
-    ]
-
-    def weights(j, d):
-        src = (w1_ref, w2_ref)[j]
-        return remote(src, wbuf.at[j, fx], w_send.at[j, d], w_recv.at[j, d], (right, left)[d])
-
-    def weights_arrival(j, d):
-        slot = wbuf.at[j, mod4(fx - 1) if d == 0 else mod4(fx + 1)]
-        return remote(slot, slot, w_send.at[j, d], w_recv.at[j, d], (right, left)[d])
-
-    def passed_on(j):
-        slot = wbuf.at[j, mod4(fx - 1) if j == 0 else mod4(fx + 1)]
-        return remote(slot, slot, w_send.at[j, 2], w_recv.at[j, 2], (right, left)[j])
-
-    def passed_arrival(j):
-        slot = wbuf.at[j, mod4(fx + 2)]
-        return remote(slot, slot, w_send.at[j, 2], w_recv.at[j, 2], (right, left)[j])
-
-    for o in owns:
-        o.start()
-    for j, d in ((0, 0), (1, 1), (1, 0), (0, 1)):
-        weights(j, d).start()
-
     for d in range(1, RING):
         pl.when(y + d < RING)(lambda: pl.semaphore_wait(ready_row.at[y + d], 1))
 
@@ -223,7 +223,14 @@
         slot = kv.at[c, maj[c], b]
         return remote(slot, slot, kv1_send.at[c, 0], kv1_recv.at[c, b], {axis_of[1 - c]: b})
 
-    for d in range(1, RING):
+    def relayed(i):
+        from_left = (i == 3) | ((i == 4) & (tp == 0))
+        block = mod8(jnp.where(from_left, y - 2, y + 2))
+        peer = mod8(y + 1) if i == 3 else mod8(y - 1) if i == 5 else mod8(jnp.where(from_left, y + 2, y - 2))
+        slot = kv.at[0, z, block]
+        return remote(slot, slot, kv1_send.at[0, i], kv1_recv.at[0, block], {"sp_1": peer})
+
+    for d in (1, 7, 2, 6):
         first(0, d).start()
 
     for d in range(1, RING):
@@ -343,6 +350,11 @@
     def up_total(d):
         return remote(tot, s2.at[z], s2_send.at[d], s2_recv.at[z], {"sp_0": z + d})
 
+    for d in (2, 6):
+        first_arrival(0, mod8(y + d)).wait_recv()
+    for i in (3, 5, 4):
+        relayed(i).start()
+
     s1_out = [around(lambda p: msg.at[p], s1, s1_send, s1_recv, "sp_1", d) for d in range(1, RING)]
     for o in s1_out:
         o.start()
@@ -434,7 +446,7 @@
 
     def arrive(c, half):
         for b in range(4 * half, 4 * half + 4):
-            there = (b != y) if c == 0 else (b < z)
+            there = (b != y) & (b != mod8(y + 2)) & (b != mod8(y - 2)) if c == 0 else (b < z)
             pl.when(there)(lambda: first_arrival(c, b).wait_recv())
         for d in range(2):
             send(c, d, half)
@@ -452,7 +464,7 @@
             passed_on(0).start()
             weights_arrival(1, 1).wait_recv()
             passed_on(1).start()
-        if k == -1:
+        if k == 0:
             for d in range(1, RING):
                 around_arrival(s1, s1_send, s1_recv, "sp_1", d).wait_recv()
             run = jnp.zeros((HD, ROWS), F32)
@@ -489,8 +501,12 @@
             u = u * silu(gate_ref[...].astype(F32))
             stretch = lax.rsqrt(jnp.mean(u * u, axis=1, keepdims=True) + EPSILON)
             xs_sc[...] = (u * stretch * gain_ref[...]).astype(BF16)
-
-    stage(-1)
+            for o in owns:
+                o.wait()
+            weights_arrival(0, 1).wait_recv()
+            for n, f in enumerate((fx, mod4(fx - 1), mod4(fx + 1))):
+                early[n] = dot(xs_sc[...], wbuf[0, f])
+
     for k in range(7):
         half_up = 0 if k == 6 else k % 2
         half_down = 1 if k == 6 else k % 2
@@ -526,33 +542,19 @@
 
     columns = (fx, mod4(fx - 1), mod4(fx + 1), mod4(fx + 2))
     for n, f in enumerate(columns):
-        if n == 0:
-            for o in owns:
-                o.wait()
-        elif n == 1:
+        if n == 1:
             weights_arrival(1, 0).wait_recv()
-        elif n == 2:
-            weights_arrival(0, 1).wait_recv()
-        else:
+        if n == 3:
             passed_arrival(0).wait_recv()
             passed_arrival(1).wait_recv()
-        merged = dot(state_out, wbuf[0, f]) + dot(attended, wbuf[1, f])
+        merged = (early[n] if n < 3 else dot(state_out, wbuf[0, f])) + dot(attended, wbuf[1, f])
         top, bottom = merged[0:half_rows], merged[half_rows:ROWS]
         give[n] = jnp.where(tp == 0, bottom, top).astype(BF16)
         across(n).start()
         keep[n] = jnp.where(tp == 0, top, bottom)
-    for n, f in enumerate(columns):
-        across(n).wait_recv()
-        ob[n] = (keep[n] + take[n].astype(F32)).astype(BF16)
-        written(n, f).start()
-    for n, f in enumerate(columns):
-        written(n, f).wait()
-
-    for n in range(FS):
-        across(n).wait_send()
     pl.when(me < RING * RING - 1)(lambda: each_halo(lambda h: h.wait_send()))
     for d in range(1, RING):
-        first(0, d).wait_send()
+        (first(0, d) if d in (1, 2, 6, 7) else relayed(d)).wait_send()
         around(lambda p: msg.at[p], s1, s1_send, s1_recv, "sp_1", d).wait_send()
         around(lambda p: back.at[p], carried, s3_send, s3_recv, "sp_1", d).wait_send()
 
@@ -568,6 +570,15 @@
         for d in range(2):
             weights(j, d).wait_send()
         passed_on(j).wait_send()
+
+    for n, f in enumerate(columns):
+        across(n).wait_recv()
+        ob[n] = (keep[n] + take[n].astype(F32)).astype(BF16)
+        written(n, f).start()
+    for n, f in enumerate(columns):
+        written(n, f).wait()
+    for n in range(FS):
+        across(n).wait_send()
 
 
 def shards(
@@ -616,6 +627,7 @@
             pltpu.VMEM((FS, ROWS // 2, 512), BF16),
             pltpu.VMEM((FS, ROWS // 2, 512), F32),
             pltpu.VMEM((FS, ROWS // 2, 512), BF16),
+            pltpu.VMEM((3, ROWS, 512), F32),
             dma((2, RING)), dma((2, RING)),
             dma((2, 2, 7)), dma((2, 2, 7)),
             dma((RING,)), dma((RING,)), dma((RING,)), dma((RING,)), dma((RING,)), dma((RING,)),

time: 57 us -> 57.5 us (level)
  the two profiles are of different devices: /device:TPU:257 before, /device:TPU:385 now
where the time goes in v5:
time: 57.5 us; the launch traced here: 57.3 us
  Pallas kernels  55.6 us (97%)
  local copies, waits for them, and re-layouts  1.67 us (3%)
    pallas_call x1, Pallas kernels, shards(): pl.pallas_call(kernel, out_shape=jax.ShapeDtypeStruct((ROWS // 2, 512 * F...  55.6 us
    unnamed x1, local copies, waits for them, and re-layouts  1.67 us

profile of v5, /device:TPU:385, one launch (start us, length us, event | category | flops | bytes accessed | tf_op | source)
XLA Modules:
  0.0 57.3 jit_solution(5098866600466793054)
XLA Ops:
  0.0 55.6 %mixer.1 = bf16[64,2048]{1,0:T(8,128)(2,1)} custom-call(bf16[128,512]{1,0:T(8,128)(2,1)} %bitcast.17, bf16[128,128]{1,0:T(8,128)(2,1)} %bitcast.20, bf16[128,128]{1,0:T(8,128)(2,1)} %bitcast.21, bf16[128,512]{1,0:T(8,128)(2,1)} %bitcast.18, f32[8,128]{1,0:T(8,128)} %bitcast.24, f32[8,128]{1,0:T(8,128)} %bitcast.25, f32[1,8]{1,0:T(1,128)} %bitcast.28, ...), custom_call_target="tpu_custom_call" | custom-call | tf_op jit(solution)/shard_map/mixer/pallas_call | solution.py:593
  55.6 1.7 %copy.20 = bf16[1,64,2048]{2,1,0:T(8,128)(2,1)} copy(bf16[1,64,2048]{2,1,0:T(8,128)(2,1)} %bitcast.16) | data formatting | bytes 524288

commit v6 on v5

--- a/solution.py
+++ b/solution.py
@@ -53,11 +53,11 @@
 def kernel(
     x_in, w_in, r_in, gate_in, step_in, extra_in, lane_in, bypass_in, xtap_in, wtap_in, rtap_in,
     gain_in, q_in, k_in, v_in, g_in, w1_ref, w2_ref,
-    out_ref,
+    keep_out, take_out,
     x_ref, w_ref, r_ref, gate_ref, step_ref, extra_ref, lane_ref, bypass_ref, xtap_ref, wtap_ref, rtap_ref,
     gain_ref, q_ref, k_ref, v_ref, g_ref,
     kv, qs, wide, hx, hw, hr, m_sc, acc_sc, msg, s1, tot, s2, pre, cumpre, back, carried,
-    xs_sc, ms_sc, rd_sc, ecum_sc, wbuf, give, take, keep, ob, early,
+    xs_sc, ms_sc, rd_sc, ecum_sc, wbuf, give, keep, early,
     kv1_send, kv1_recv, kv_send, kv_recv, s1_send, s1_recv, s2_send, s2_recv, s3_send, s3_recv,
     w_send, w_recv, own_sem, halo_send, halo_recv, tp_send, tp_recv, in_sem, out_sem, ready, ready_row,
 ):
@@ -479,7 +479,7 @@
             tot[HD:MSG] = decay_rows(jnp.broadcast_to(total, (8, ROWS)))
             for d in range(1, RING):
                 pl.when(z + d < RING)(lambda: up_total(d).start())
-        if k == 2:
+        if k == 4:
             for j in range(RING - 1):
                 slot = s2.at[j]
                 come = remote(slot, slot, s2_send.at[0], s2_recv.at[j], {"sp_0": j})
@@ -493,7 +493,7 @@
             for d in range(1, RING):
                 around(lambda p: back.at[p], carried, s3_send, s3_recv, "sp_1", d).start()
             carried[y] = back[y]
-        if k == 5:
+        if k == 6:
             for d in range(1, RING):
                 around_arrival(carried, s3_send, s3_recv, "sp_1", d).wait_recv()
             states = jnp.concatenate([carried[h] for h in range(8)], axis=0)
@@ -532,13 +532,13 @@
     state_out = xs_sc[...]
     half_rows = ROWS // 2
 
-    def across(n):
-        return remote(give.at[n], take.at[n], tp_send.at[n], tp_recv.at[n], {"tp": 1 - tp})
+    def across(n, f):
+        slot = take_out.at[:, pl.ds(pl.multiple_of(512 * f, 512), 512)]
+        return remote(give.at[n], slot, tp_send.at[n], tp_recv.at[n], {"tp": 1 - tp})
 
     def written(n, f):
-        return pltpu.make_async_copy(
-            ob.at[n], out_ref.at[:, pl.ds(pl.multiple_of(512 * f, 512), 512)], out_sem.at[n]
-        )
+        slot = keep_out.at[:, pl.ds(pl.multiple_of(512 * f, 512), 512)]
+        return pltpu.make_async_copy(keep.at[n], slot, out_sem.at[n])
 
     columns = (fx, mod4(fx - 1), mod4(fx + 1), mod4(fx + 2))
     for n, f in enumerate(columns):
@@ -550,8 +550,9 @@
         merged = (early[n] if n < 3 else dot(state_out, wbuf[0, f])) + dot(attended, wbuf[1, f])
         top, bottom = merged[0:half_rows], merged[half_rows:ROWS]
         give[n] = jnp.where(tp == 0, bottom, top).astype(BF16)
-        across(n).start()
         keep[n] = jnp.where(tp == 0, top, bottom)
+        across(n, f).start()
+        written(n, f).start()
     pl.when(me < RING * RING - 1)(lambda: each_halo(lambda h: h.wait_send()))
     for d in range(1, RING):
         (first(0, d) if d in (1, 2, 6, 7) else relayed(d)).wait_send()
@@ -572,13 +573,9 @@
         passed_on(j).wait_send()
 
     for n, f in enumerate(columns):
-        across(n).wait_recv()
-        ob[n] = (keep[n] + take[n].astype(F32)).astype(BF16)
-        written(n, f).start()
-    for n, f in enumerate(columns):
         written(n, f).wait()
-    for n in range(FS):
-        across(n).wait_send()
+        across(n, f).wait_send()
+        across(n, f).wait_recv()
 
 
 def shards(
@@ -590,11 +587,14 @@
 ):
     hbm = pl.BlockSpec(memory_space=pltpu.HBM)
     dma = pltpu.SemaphoreType.DMA
-    out = pl.pallas_call(
+    kept, taken = pl.pallas_call(
         kernel,
-        out_shape=jax.ShapeDtypeStruct((ROWS // 2, 512 * FS), BF16),
+        out_shape=(
+            jax.ShapeDtypeStruct((ROWS // 2, 512 * FS), F32),
+            jax.ShapeDtypeStruct((ROWS // 2, 512 * FS), BF16),
+        ),
         in_specs=[hbm] * 18,
-        out_specs=hbm,
+        out_specs=(hbm, hbm),
         scratch_shapes=[
             pltpu.VMEM((ROWS, 512), BF16), pltpu.VMEM((ROWS, ROWS), BF16), pltpu.VMEM((ROWS, ROWS), BF16),
             pltpu.VMEM((ROWS, 512), BF16), pltpu.VMEM((8, ROWS), F32), pltpu.VMEM((8, ROWS), F32),
@@ -624,9 +624,7 @@
             pltpu.VMEM((ROWS, 512), F32),
             pltpu.VMEM((2, FS, 512, 512), BF16),
             pltpu.VMEM((FS, ROWS // 2, 512), BF16),
-            pltpu.VMEM((FS, ROWS // 2, 512), BF16),
             pltpu.VMEM((FS, ROWS // 2, 512), F32),
-            pltpu.VMEM((FS, ROWS // 2, 512), BF16),
             pltpu.VMEM((3, ROWS, 512), F32),
             dma((2, RING)), dma((2, RING)),
             dma((2, 2, 7)), dma((2, 2, 7)),
@@ -647,7 +645,7 @@
         bundled_rescaling_vector.reshape(1, -1), queries[0], attention_keys[0], attention_values[0],
         forget_gate_cumsum[0].T, state_out_weight, attention_out_weight,
     )
-    return out[None]
+    return (kept + taken.astype(F32)).astype(BF16)[None]
 
 
 def solution(mesh):

time: 57.5 us -> 55.6 us (0.967)
  the two profiles are of different devices: /device:TPU:385 before, /device:TPU:273 now
where the time goes in v6:
time: 55.6 us; the launch traced here: 55.4 us
  Pallas kernels  53.6 us (96%)
  other arithmetic  1.86 us (3%)
    pallas_call x1, Pallas kernels, shards(): pl.pallas_call(kernel, out_shape=(jax.ShapeDtypeStruct((ROWS // 2, 512 *...  53.6 us
    broadcast_in_dim x1, other arithmetic, shards(): return (kept + taken.astype(F32)).astype(BF16)[None]  1.86 us

profile of v6, /device:TPU:273, one launch (start us, length us, event | category | flops | bytes accessed | tf_op | source)
XLA Modules:
  0.0 55.4 jit_solution(186736501055614565)
XLA Ops:
  0.0 53.6 %mixer.1 = (f32[64,2048]{1,0:T(8,128)}, bf16[64,2048]{1,0:T(8,128)(2,1)}) custom-call(bf16[128,512]{1,0:T(8,128)(2,1)} %bitcast.17, bf16[128,128]{1,0:T(8,128)(2,1)} %bitcast.20, bf16[128,128]{1,0:T(8,128)(2,1)} %bitcast.21, bf16[128,512]{1,0:T(8,128)(2,1)} %bitcast.18, f32[8,128]{1,0:T(8,128)} %bitcast.24, f32[8,128]{1,0:T(8,128)} %bitcast.25, ...), custom_call_target="tpu_custom_call" | custom-call | tf_op jit(solution)/shard_map/mixer/pallas_call | solution.py:590
  53.6 1.9 %fusion = bf16[1,64,2048]{2,1,0:T(8,128)(2,1)} fusion(f32[64,2048]{1,0:T(8,128)} %get-tuple-element.7, bf16[64,2048]{1,0:T(8,128)(2,1)} %get-tuple-element.8), kind=kLoop, calls=%fused_computation.1 | loop fusion | flops 393216 | bytes 1048576 | tf_op jit(solution)/shard_map/broadcast_in_dim | solution.py:648

commit v7 on v6

--- a/solution.py
+++ b/solution.py
@@ -161,7 +161,7 @@
         weights(j, d).start()
 
     wide[...] = jnp.zeros_like(wide)
-    for copy in ins[0:4]:
+    for copy in ins[0:4] + ins[7:10]:
         copy.wait()
     kf, vt = k_ref[...].astype(F32), v_ref[...].astype(F32).T
     low64 = low[0:HD]
@@ -171,9 +171,22 @@
     )
     hi, mid, lo = split3(-g_ref[...])
     four = sub8 < 4
+    raw = step_ref[...]
+    step = jnp.maximum(raw, 0.0) + jnp.log1p(jnp.exp(-jnp.abs(raw)))
+    on_diagonal = sub8[:, 0:8] == lax.broadcasted_iota(jnp.int32, (8, 8), 1)
+    rate = jnp.sum(jnp.where(on_diagonal, lane_ref[...], 0.0), axis=1, keepdims=True)
+    cum = step * (-jnp.exp(rate)) + extra_ref[...]
+    lane8 = lax.broadcasted_iota(jnp.int32, (8, ROWS), 1)
+    for shift in (1, 2, 4, 8, 16, 32, 64):
+        cum = cum + jnp.where(lane8 >= shift, pltpu.roll(cum, shift, 1), 0.0)
+    end = cum[:, ROWS - 1 : ROWS]
+    ends = jnp.sum(jnp.where(sub8 == lane8, end, 0.0), axis=0, keepdims=True)
+    spare = jnp.zeros((8, ROWS), F32)
+    for i, piece in enumerate(split3(ends)):
+        spare = jnp.where(sub8 == 4 + i, piece, spare)
     gate_rows = (
         jnp.concatenate(
-            [jnp.where(four, hi, pltpu.roll(lo, 4, 0)), jnp.where(four, mid, 0.0)], axis=0
+            [jnp.where(four, hi, pltpu.roll(lo, 4, 0)), jnp.where(four, mid, spare)], axis=0
         ),
         jnp.concatenate(
             [jnp.where(four, pltpu.roll(hi, 4, 0), lo), jnp.where(four, pltpu.roll(mid, 4, 0), 0.0)],
@@ -190,7 +203,8 @@
         qf = q_ref[:, 128 * p : 128 * p + 128].astype(F32) * 0.125
         turn = pltpu.roll(qf, HD, 1)
         at = slice(ROWS * e, ROWS * e + ROWS)
-        picks = jnp.where(lax.rem(lane, 4) == h % 4, 1.0, 0.0).astype(BF16)
+        picks = (lax.rem(lane, 4) == h % 4) & (lax.rem(lane, 16) < 12)
+        picks = jnp.where(picks, 1.0, 0.0).astype(BF16)
         head, other = (qf, turn) if e == 0 else (turn, qf)
         qs[p, 0, at, 0:ROWS] = jnp.where(low, head, 0.0).astype(BF16)
         qs[p, 1, at, 0:ROWS] = jnp.where(low, 0.0, other).astype(BF16)
@@ -267,7 +281,7 @@
             m_sc[p] = jnp.broadcast_to(m, (8, 2 * ROWS))
             acc_sc[p] = dot(vals, probs)
 
-    for copy in ins[7:]:
+    for copy in ins[10:]:
         copy.wait()
 
     @pl.when(me > 0)
@@ -289,15 +303,6 @@
     wr = filtered(w_ref, hw, wtap_ref)
     rd = filtered(r_ref, hr, rtap_ref)
     rd_sc[...] = rd
-    raw = step_ref[...]
-    step = jnp.maximum(raw, 0.0) + jnp.log1p(jnp.exp(-jnp.abs(raw)))
-    on_diagonal = sub8[:, 0:8] == lax.broadcasted_iota(jnp.int32, (8, 8), 1)
-    rate = jnp.sum(jnp.where(on_diagonal, lane_ref[...], 0.0), axis=1, keepdims=True)
-    cum = step * (-jnp.exp(rate)) + extra_ref[...]
-    lane8 = lax.broadcasted_iota(jnp.int32, (8, ROWS), 1)
-    for shift in (1, 2, 4, 8, 16, 32, 64):
-        cum = cum + jnp.where(lane8 >= shift, pltpu.roll(cum, shift, 1), 0.0)
-    end = cum[:, ROWS - 1 : ROWS]
     scale = jnp.exp(end - cum) * step
     wide[0:8] = cum
     wide[8:16] = scale
@@ -323,7 +328,7 @@
         state = dot((xf * ends).astype(BF16), wr, TN)
         for e in range(2):
             h = 2 * p + e
-            msg[h, 0:HD] = state[HD * e : HD * e + HD].astype(BF16)
+            msg[h] = state[HD * e : HD * e + HD].astype(BF16)
 
     def decay_rows(total):
         a, b, c3 = split3(total)
@@ -332,9 +337,6 @@
     def decay_of(rows):
         f = rows.astype(F32)
         return (f[0:1] + f[8:9]) + f[4:5]
-
-    for h in range(8):
-        msg[h, HD:MSG] = decay_rows(jnp.broadcast_to(end[h : h + 1], (8, ROWS)))
 
     def around(src, dst, send, recv, axis, d):
         me_on = y if axis == "sp_1" else z
@@ -472,8 +474,11 @@
             for j in range(RING):
                 pre[j] = run
                 cumpre[j] = jnp.broadcast_to(total, (8, ROWS))
-                ld = decay_of(s1[j, HD:MSG])
-                run = jnp.exp(ld) * run + s1[j, 0:HD].astype(F32)
+                g = kv[0, z, j, ROWS:BLOCK].astype(F32)
+                ld = (g[12:13] + g[13:14]) + g[14:15]
+                ld = jnp.sum(jnp.where(lane[0:1] == y, ld, 0.0), axis=1, keepdims=True)
+                ld = jnp.broadcast_to(ld, (1, ROWS))
+                run = jnp.exp(ld) * run + s1[j].astype(F32)
                 total = total + ld
             tot[0:HD] = run.astype(BF16)
             tot[HD:MSG] = decay_rows(jnp.broadcast_to(total, (8, ROWS)))
@@ -510,7 +515,7 @@
     for k in range(7):
         half_up = 0 if k == 6 else k % 2
         half_down = 1 if k == 6 else k % 2
-        for c in (1, 0):
+        for c in (0, 1):
             for d in range(2):
                 pl.when(coming(c, d, k))(lambda: hop_arrival(c, d, k).wait_recv())
             if k < 5:
@@ -610,8 +615,8 @@
             pltpu.VMEM((16, ROWS), BF16),
             pltpu.VMEM((4, 8, 2 * ROWS), F32),
             pltpu.VMEM((4, HD + 16, 2 * ROWS), F32),
-            pltpu.VMEM((RING, MSG, ROWS), BF16),
-            pltpu.VMEM((RING, MSG, ROWS), BF16),
+            pltpu.VMEM((RING, HD, ROWS), BF16),
+            pltpu.VMEM((RING, HD, ROWS), BF16),
             pltpu.VMEM((MSG, ROWS), BF16),
             pltpu.VMEM((RING, MSG, ROWS), BF16),
             pltpu.VMEM((RING, HD, ROWS), F32),

time: 55.6 us -> 55.6 us (level)
  the two profiles are of different devices: /device:TPU:273 before, /device:TPU:193 now
where the time goes in v7:
time: 55.6 us; the launch traced here: 55.4 us
  Pallas kernels  53.6 us (96%)
  other arithmetic  1.86 us (3%)
    pallas_call x1, Pallas kernels, shards(): pl.pallas_call(kernel, out_shape=(jax.ShapeDtypeStruct((ROWS // 2, 512 *...  53.6 us
    broadcast_in_dim x1, other arithmetic, shards(): return (kept + taken.astype(F32)).astype(BF16)[None]  1.86 us

profile of v7, /device:TPU:193, one launch (start us, length us, event | category | flops | bytes accessed | tf_op | source)
XLA Modules:
  0.0 55.4 jit_solution(17501440371953267725)
XLA Ops:
  0.0 53.6 %mixer.1 = (f32[64,2048]{1,0:T(8,128)}, bf16[64,2048]{1,0:T(8,128)(2,1)}) custom-call(bf16[128,512]{1,0:T(8,128)(2,1)} %bitcast.17, bf16[128,128]{1,0:T(8,128)(2,1)} %bitcast.20, bf16[128,128]{1,0:T(8,128)(2,1)} %bitcast.21, bf16[128,512]{1,0:T(8,128)(2,1)} %bitcast.18, f32[8,128]{1,0:T(8,128)} %bitcast.24, f32[8,128]{1,0:T(8,128)} %bitcast.25, ...), custom_call_target="tpu_custom_call" | custom-call | tf_op jit(solution)/shard_map/mixer/pallas_call | solution.py:595
  53.6 1.9 %fusion = bf16[1,64,2048]{2,1,0:T(8,128)(2,1)} fusion(f32[64,2048]{1,0:T(8,128)} %get-tuple-element.7, bf16[64,2048]{1,0:T(8,128)(2,1)} %get-tuple-element.8), kind=kLoop, calls=%fused_computation.1 | loop fusion | flops 393216 | bytes 1048576 | tf_op jit(solution)/shard_map/broadcast_in_dim | solution.py:653

commit v8 on v7

--- a/solution.py
+++ b/solution.py
@@ -460,6 +460,21 @@
     arrive(0, 1)
     attend(0, 0, 0, 0, 1)
 
+    def entering_states():
+        for j in range(RING - 1):
+            slot = s2.at[j]
+            come = remote(slot, slot, s2_send.at[0], s2_recv.at[j], {"sp_0": j})
+            pl.when(j < z)(lambda: come.wait_recv())
+        entering = jnp.zeros((HD, ROWS), F32)
+        for j in range(RING - 1):
+            later = jnp.exp(decay_of(s2[j, HD:MSG])) * entering + s2[j, 0:HD].astype(F32)
+            entering = jnp.where(j < z, later, entering)
+        for j in range(RING):
+            back[j] = (pre[j] + jnp.exp(cumpre[j, 0:1]) * entering).astype(BF16)
+        for d in range(1, RING):
+            around(lambda p: back.at[p], carried, s3_send, s3_recv, "sp_1", d).start()
+        carried[y] = back[y]
+
     def stage(k):
         if k == 0:
             weights_arrival(0, 0).wait_recv()
@@ -484,20 +499,10 @@
             tot[HD:MSG] = decay_rows(jnp.broadcast_to(total, (8, ROWS)))
             for d in range(1, RING):
                 pl.when(z + d < RING)(lambda: up_total(d).start())
+        if k == 2:
+            pl.when(z < 4)(entering_states)
         if k == 4:
-            for j in range(RING - 1):
-                slot = s2.at[j]
-                come = remote(slot, slot, s2_send.at[0], s2_recv.at[j], {"sp_0": j})
-                pl.when(j < z)(lambda: come.wait_recv())
-            entering = jnp.zeros((HD, ROWS), F32)
-            for j in range(RING - 1):
-                later = jnp.exp(decay_of(s2[j, HD:MSG])) * entering + s2[j, 0:HD].astype(F32)
-                entering = jnp.where(j < z, later, entering)
-            for j in range(RING):
-                back[j] = (pre[j] + jnp.exp(cumpre[j, 0:1]) * entering).astype(BF16)
-            for d in range(1, RING):
-                around(lambda p: back.at[p], carried, s3_send, s3_recv, "sp_1", d).start()
-            carried[y] = back[y]
+            pl.when(z >= 4)(entering_states)
         if k == 6:
             for d in range(1, RING):
                 around_arrival(carried, s3_send, s3_recv, "sp_1", d).wait_recv()

time: 55.6 us -> 55.1 us (level)
  the two profiles are of different devices: /device:TPU:193 before, /device:TPU:385 now
where the time goes in v8:
time: 55.1 us; the launch traced here: 54.8 us
  Pallas kernels  53 us (96%)
  other arithmetic  1.86 us (3%)
    pallas_call x1, Pallas kernels, shards(): pl.pallas_call(kernel, out_shape=(jax.ShapeDtypeStruct((ROWS // 2, 512 *...  53 us
    broadcast_in_dim x1, other arithmetic, shards(): return (kept + taken.astype(F32)).astype(BF16)[None]  1.86 us

profile of v8, /device:TPU:385, one launch (start us, length us, event | category | flops | bytes accessed | tf_op | source)
XLA Modules:
  0.0 54.8 jit_solution(4778815068729756656)
XLA Ops:
  0.0 53.0 %mixer.1 = (f32[64,2048]{1,0:T(8,128)}, bf16[64,2048]{1,0:T(8,128)(2,1)}) custom-call(bf16[128,512]{1,0:T(8,128)(2,1)} %bitcast.17, bf16[128,128]{1,0:T(8,128)(2,1)} %bitcast.20, bf16[128,128]{1,0:T(8,128)(2,1)} %bitcast.21, bf16[128,512]{1,0:T(8,128)(2,1)} %bitcast.18, f32[8,128]{1,0:T(8,128)} %bitcast.24, f32[8,128]{1,0:T(8,128)} %bitcast.25, ...), custom_call_target="tpu_custom_call" | custom-call | tf_op jit(solution)/shard_map/mixer/pallas_call | solution.py:600
  53.0 1.9 %fusion = bf16[1,64,2048]{2,1,0:T(8,128)(2,1)} fusion(f32[64,2048]{1,0:T(8,128)} %get-tuple-element.7, bf16[64,2048]{1,0:T(8,128)(2,1)} %get-tuple-element.8), kind=kLoop, calls=%fused_computation.1 | loop fusion | flops 393216 | bytes 1048576 | tf_op jit(solution)/shard_map/broadcast_in_dim | solution.py:658
